TPU v7x, 32 devices: a whole 2x2x4 slice. The times are simulated.
32 devices in a mesh: kv: 8 (over z, core), tp: 4 (over y, x).
Axes of the slice: x: 2, y: 2, z: 4, core: 2. Of those that a mesh axis runs over, the one named last changes fastest.
Arguments:
- tokens: bfloat16 [16, 2048], P(None, 'kv'), may hold values from -8 to 8
- lengths: int32 [16], replicated, may hold values from 1 to 3072, 12288 in all
- latent_cache: bfloat16 [16, 3072, 256], P(None, ('kv', 'tp')), may hold values from -10 to 10
- rope_cache: bfloat16 [16, 3072, 32], P(None, ('kv', 'tp')), may hold values from -2000 to 2000
- gain_in: bfloat16 [2048], P('kv'), may hold values from 0.099609375 to 1.8984375
- w_down_q: bfloat16 [2048, 512], P('kv'), may hold values from -0.125 to 0.125
- w_down_kv: bfloat16 [2048, 256], P('kv'), may hold values from -0.125 to 0.125
- w_rope_key: bfloat16 [2048, 32], P('kv'), may hold values from -0.125 to 0.125
- gain_q: bfloat16 [512], replicated, may hold values from 0.099609375 to 1.8984375
- w_up_qn: bfloat16 [512, 16, 64], replicated, may hold values from -0.25 to 0.25
- w_up_qr: bfloat16 [512, 16, 32], replicated, may hold values from -0.25 to 0.25
- gain_kv: bfloat16 [256], replicated, may hold values from 0.099609375 to 1.8984375
- w_key_up: bfloat16 [256, 16, 64], replicated, may hold values from -0.375 to 0.375
- w_value_up: bfloat16 [256, 16, 64], replicated, may hold values from -0.375 to 0.375
- w_attn_out: bfloat16 [16, 64, 2048], P('tp', None, 'kv'), may hold values from -0.1875 to 0.1875
- gain_mid: bfloat16 [2048], P('kv'), may hold values from 0.099609375 to 1.8984375
- w_ff_in: bfloat16 [2048, 8192], P('kv', 'tp'), may hold values from -0.125 to 0.125
- w_ff_out: bfloat16 [8192, 2048], P('tp', 'kv'), may hold values from -0.0625 to 0.0625
Outputs:
- mixed: bfloat16 [16, 2048], P(None, 'kv')
- new_latent: bfloat16 [16, 256], replicated
- new_rope_key: bfloat16 [16, 32], replicated
Inputs may be any that keep to these rules, and one draw needn't show every extreme that they name: `lengths`: each sequence's live cache positions; one sequence fills the whole cache.
All inputs are finite; a program needn't handle non-finite values.
Results may differ from a plain program's by a relative error of at most 0.012.
Values sent between devices are 32-bit elements; how exact they have to be, the bound alone decides.
No kernel may reach another device: no remote copies, remote signals or barrier semaphores. Data moves between devices by JAX's collectives and lax.ppermute only.
A program may use at most 64 MiB of HBM per device.

v0:
```python
import jax
import jax.numpy as jnp
from jax import lax
from jax.sharding import PartitionSpec as P

D = 2048
NOPE = 64
ROPE = 32


EPS = 1e-06


def combined_all(part, axis, combine):
    gathered = jax.tree.map(lambda a: lax.all_gather(a, axis), part)

    def take(source):
        return jax.tree.map(lambda a: lax.dynamic_index_in_dim(a, source, 0, False), gathered)

    return lax.fori_loop(
        1, lax.axis_size(axis), lambda source, state: combine(state, take(source)), take(0)
    )


def rotate(values, positions):
    half = values.shape[-1] // 2
    inverse = 10000.0 ** (-jnp.arange(half, dtype=jnp.float32) / half)
    angle = positions.astype(jnp.float32)[:, None, None] * inverse[None, None, :]
    first = values[..., :half]
    second = values[..., half:]
    return jnp.concatenate(
        [
            first * jnp.cos(angle) - second * jnp.sin(angle),
            second * jnp.cos(angle) + first * jnp.sin(angle),
        ],
        axis=-1,
    )


def rms_scaled(values, gain):
    return (
        values
        * lax.rsqrt(jnp.mean(values * values, axis=-1, keepdims=True) + EPS)
        * gain.astype(jnp.float32)
    )


def combine(earlier, later):
    top_a, total_a, acc_a = earlier
    top_b, total_b, acc_b = later
    top = jnp.maximum(top_a, top_b)
    fade_a = jnp.exp(top_a - top)
    fade_b = jnp.exp(top_b - top)
    return (
        top,
        total_a * fade_a + total_b * fade_b,
        acc_a * fade_a[..., None] + acc_b * fade_b[..., None],
    )


def fold_sources(parts):
    tops, totals, accs = parts
    top = jnp.max(tops, axis=0)
    fade = jnp.exp(tops - top[None])
    return (top, jnp.sum(totals * fade, axis=0), jnp.sum(accs * fade[..., None], axis=0))


def per_device(
    tokens,
    lengths,
    latent_cache,
    rope_cache,
    gain_in,
    w_down_q,
    w_down_kv,
    w_rope_key,
    gain_q,
    w_up_qn,
    w_up_qr,
    gain_kv,
    w_key_up,
    w_value_up,
    w_attn_out,
    gain_mid,
    w_ff_in,
    w_ff_out,
):
    f32 = jnp.float32
    bf16 = jnp.bfloat16
    highest = lax.Precision.HIGHEST
    scale = (NOPE + ROPE) ** (-0.5)
    resid = tokens.astype(f32)
    scaled_in = (resid * gain_in.astype(f32)).astype(bf16)
    part_q = jnp.dot(scaled_in, w_down_q, preferred_element_type=f32)
    part_kv = jnp.dot(scaled_in, w_down_kv, preferred_element_type=f32)
    part_rope = jnp.dot(scaled_in, w_rope_key, preferred_element_type=f32)
    square_in = jnp.sum(resid * resid, axis=1)
    sum_q, sum_kv, sum_rope, total_in = lax.psum((part_q, part_kv, part_rope, square_in), "kv")
    inv_in = lax.rsqrt(total_in / D + EPS)[:, None]
    query_latent = rms_scaled(inv_in * sum_q, gain_q).astype(bf16)
    new_latent = rms_scaled(inv_in * sum_kv, gain_kv).astype(bf16)
    new_rope_key = rotate((inv_in * sum_rope)[:, None, :], lengths)[:, 0, :].astype(bf16)
    query_nope = jnp.einsum(
        "bc,chd->bhd", query_latent, w_up_qn, preferred_element_type=f32
    ).astype(bf16)
    query_rope = rotate(
        jnp.einsum("bc,chr->bhr", query_latent, w_up_qr, preferred_element_type=f32), lengths
    ).astype(bf16)
    query_cache = jnp.einsum(
        "bhd,khd->bhk", query_nope, w_key_up, preferred_element_type=f32
    ).astype(bf16)
    rows = latent_cache.shape[1]
    positions = lax.axis_index(("kv", "tp")) * rows + jnp.arange(rows, dtype=jnp.int32)
    live = (positions[None, :] < lengths[:, None])[:, None, :]
    scores = (
        jnp.einsum("bhk,blk->bhl", query_cache, latent_cache, preferred_element_type=f32)
        + jnp.einsum("bhr,blr->bhl", query_rope, rope_cache, preferred_element_type=f32)
    ) * scale
    scores = jnp.where(live, scores, -1e30)
    top = jnp.max(scores, axis=2)
    weights = jnp.where(live, jnp.exp(scores - top[:, :, None]), 0.0)
    total = jnp.sum(weights, axis=2)
    acc = jnp.einsum("bhl,blk->bhk", weights.astype(bf16), latent_cache, preferred_element_type=f32)
    heads_dev = w_attn_out.shape[0]
    first_head = lax.axis_index("tp") * heads_dev
    own_value_up = lax.dynamic_slice_in_dim(w_value_up, first_head, heads_dev, 1).astype(f32)
    own_cache_q = lax.dynamic_slice_in_dim(query_cache, first_head, heads_dev, 1)
    own_rope_q = lax.dynamic_slice_in_dim(query_rope, first_head, heads_dev, 1)
    self_score = (
        jnp.einsum("bhk,bk->bh", own_cache_q, new_latent, preferred_element_type=f32)
        + jnp.einsum("bhr,br->bh", own_rope_q, new_rope_key, preferred_element_type=f32)
    ) * scale
    top, total, acc = fold_sources(
        (
            lax.all_to_all(top[None], "tp", split_axis=2, concat_axis=0, tiled=True),
            lax.all_to_all(total[None], "tp", split_axis=2, concat_axis=0, tiled=True),
            lax.all_to_all(acc[None], "tp", split_axis=2, concat_axis=0, tiled=True),
        )
    )
    top, total, acc = combined_all((top, total, acc), "kv", combine)
    joined = jnp.maximum(top, self_score)
    fade = jnp.exp(top - joined)
    self_weight = jnp.exp(self_score - joined)
    total = total * fade + self_weight
    acc = (
        acc * fade[:, :, None]
        + self_weight.astype(bf16).astype(f32)[:, :, None] * new_latent.astype(f32)[:, None, :]
    )
    expanded = jnp.einsum("bhk,khv->bhv", acc, own_value_up, precision=highest)
    head_out = (expanded / total[:, :, None]).astype(bf16)
    attn_part = jnp.einsum("bhv,hvd->bd", head_out, w_attn_out, preferred_element_type=f32)
    resid_mid = resid + lax.psum(attn_part, "tp")
    scaled_mid = (resid_mid * gain_mid.astype(f32)).astype(bf16)
    hidden_part = jnp.dot(scaled_mid, w_ff_in, preferred_element_type=f32)
    square_mid = jnp.sum(resid_mid * resid_mid, axis=1)
    hidden_sum, total_mid = lax.psum((hidden_part, square_mid), "kv")
    inv_mid = lax.rsqrt(total_mid / D + EPS)[:, None]
    hidden = jnp.square(jax.nn.relu(inv_mid * hidden_sum)).astype(bf16)
    out_part = jnp.dot(hidden, w_ff_out, preferred_element_type=f32)
    mixed = (resid_mid + lax.psum(out_part, "tp")).astype(bf16)
    return (mixed, new_latent, new_rope_key)


def solution(mesh):
    return jax.shard_map(
        per_device,
        mesh=mesh,
        in_specs=(
            P(None, "kv"),
            P(),
            P(None, ("kv", "tp"), None),
            P(None, ("kv", "tp"), None),
            P("kv"),
            P("kv", None),
            P("kv", None),
            P("kv", None),
            P(),
            P(),
            P(),
            P(),
            P(),
            P(),
            P("tp", None, "kv"),
            P("kv"),
            P("kv", "tp"),
            P("tp", "kv"),
        ),
        out_specs=(P(None, "kv"), P(), P()),
        check_vma=False,
    )
```

profile of v0, /device:TPU:0, one launch (start us, length us, event | category | flops | bytes accessed | tf_op | source)
XLA Modules:
  0.0 218.2 jit_solution(16655276583001931939)
XLA Ops:
  7.2 0.8 convert_element_type.75
  8.0 0.8 fusion.23
  8.8 0.7 convert_element_type.68
  9.5 0.7 broadcast_compare_fusion
  10.2 0.7 convert_element_type.70
  10.9 0.9 fusion.41
  11.7 1.1 fusion.43
  12.8 1.2 fusion.45
  14.0 30.8 %all-reduce = (f32[16,512]{1,0:T(8,128)S(1)}, f32[16]{0:T(128)S(1)}, f32[16,256]{1,0:T(8,128)S(1)}, f32[16,32]{1,0:T(8,128)S(1)}) all-reduce(f32[16,512]{1,0:T(8,128)S(1)} %fusion.45, f32[16]{0:T(128)S(1)} %fusion.23, f32[16,256]{1,0:T(8,128)S(1)} %fusion.43, f32[16,32]{1,0:T(8,128)S(1)} %fusion.41), channel_id=1, replica_groups=mesh['kv'=8,'tp'=4] {'kv'}, use_global_device_ids=true, to_apply=%region_2.0 | all-reduce | flops 12816 | bytes 102528 | tf_op jit(solution)/shard_map/psum | solution.py:98
  44.8 0.2 multiply_reduce_fusion.1
  45.1 0.5 fusion.55
  45.6 0.7 convolution_convert_fusion
  46.5 0.1 fusion.14
  46.7 0.8 copy-done.1
  47.4 0.4 fusion.62
  47.8 0.7 copy.50
  48.5 3.7 %all-to-all-start = ((f32[1,16,16]{1,0,2:T(1,128)}), f32[1,16,16]{1,0,2:T(1,128)S(1)}, u32[]{:S(2)}, u32[]{:S(2)}) async-start(f32[1,16,16]{1,0,2:T(1,128)} %copy.50), calls=%async_computation | async-start | bytes 16384 | tf_op jit(solution)/shard_map/all_to_all | solution.py:135
  52.3 0.6 copy-done.10
  53.1 0.2 multiply_reduce_fusion.3
  53.3 0.3 convolution_bitcast_fusion
  53.6 0.7 fusion.52
  54.5 0.5 copy-done.9
  55.0 0.2 fusion.10
  55.3 0.6 copy-done.11
  56.1 0.7 copy.51
  56.8 0.8 copy.52
  57.6 4.2 %all-to-all-start.1 = ((f32[1,16,16]{1,0,2:T(1,128)}), f32[1,16,16]{1,0,2:T(1,128)S(1)}, u32[]{:S(2)}, u32[]{:S(2)}) async-start(f32[1,16,16]{1,0,2:T(1,128)} %copy.51), calls=%async_computation.1 | async-start | bytes 16384 | tf_op jit(solution)/shard_map/all_to_all | solution.py:136
  61.8 12.8 %all-gather.3 = f32[8,16,4]{1,2,0:T(4,128)S(1)} all-gather(f32[1,16,4]{1,2,0:T(4,128)S(1)} %bitcast.113), channel_id=2, replica_groups=mesh['kv'=8,'tp'=4] {'kv'}, dimensions={0}, use_global_device_ids=true | all-gather | bytes 2304 | tf_op jit(solution)/shard_map/all_gather | solution.py:15
  74.6 4.2 %all-to-all-start.2 = ((f32[1,16,16,256]{3,1,0,2:T(8,128)}), f32[1,16,16,256]{3,1,0,2:T(8,128)S(1)}, u32[]{:S(2)}, u32[]{:S(2)}) async-start(f32[1,16,16,256]{3,1,0,2:T(8,128)} %copy.52), calls=%async_computation.2 | async-start | bytes 524288 | tf_op jit(solution)/shard_map/all_to_all | solution.py:137
  78.8 12.8 %all-gather.4 = f32[8,16,4]{1,2,0:T(4,128)S(1)} all-gather(f32[1,16,4]{1,2,0:T(4,128)S(1)} %bitcast.114), channel_id=3, replica_groups=mesh['kv'=8,'tp'=4] {'kv'}, dimensions={0}, use_global_device_ids=true | all-gather | bytes 2304 | tf_op jit(solution)/shard_map/all_gather | solution.py:15
  91.8 15.1 %all-gather.2 = f32[128,4,256]{2,1,0:T(4,128)S(1)} all-gather(f32[16,4,256]{2,1,0:T(4,128)S(1)} %copy.53), channel_id=4, replica_groups=mesh['kv'=8,'tp'=4] {'kv'}, dimensions={0}, use_global_device_ids=true | all-gather | bytes 589824 | tf_op jit(solution)/shard_map/all_gather | solution.py:15
  106.8 2.5 %while.19 = (s32[]{:T(128)}, f32[16,4]{0,1:T(4,128)S(1)}, f32[16,4]{0,1:T(4,128)S(1)}, f32[16,4,256]{2,1,0:T(4,128)S(1)}, f32[8,16,4]{1,2,0:T(4,128)S(1)}, /*ind...) while((s32[]{:T(128)}, f32[16,4]{0,1:T(4,128)S(1)}, ...), condition=%wide.region_10.11_spmd, body=%wide.region_9.10_spmd.sunk | while | flops 49541 | bytes 200335 | solution.py:20
  107.0 0.1 fusion.79
  107.4 0.1 fusion.79
  107.8 0.1 fusion.79
  108.1 0.1 fusion.79
  108.5 0.1 fusion.79
  108.8 0.1 fusion.79
  109.2 0.1 fusion.79
  109.6 1.2 fusion.6
  110.8 0.2 convolution_bitcast_fusion.2
  111.0 16.5 %psum.60 = f32[16,256]{1,0:T(8,128)S(1)} all-reduce(f32[16,256]{1,0:T(8,128)S(1)} %convolution_bitcast_fusion.2), channel_id=1, replica_groups=mesh['kv'=8,'tp'=4] {'tp'}, use_global_device_ids=true, to_apply=%region_14.15 | all-reduce | flops 4096 | bytes 32768 | tf_op jit(solution)/shard_map/psum | solution.py:152
  127.6 13.6 %psum.61 = f32[16]{0:T(128)S(1)} all-reduce(f32[16]{0:T(128)S(1)} %multiply_reduce_fusion.2), channel_id=1, replica_groups=mesh['kv'=8,'tp'=4] {'kv'}, use_global_device_ids=true, to_apply=%region_16.17 | all-reduce | flops 16 | bytes 128 | tf_op jit(solution)/shard_map/psum | solution.py:156
  141.2 0.9 fusion.38
  142.2 51.4 %all-reduce.3.cloned.1.call-done = f32[16,2048]{1,0:T(8,128)} async-done(((f32[16,2048]{1,0:T(8,128)}), f32[16,2048]{1,0:T(8,128)}) %all-reduce.3.cloned.1.call-update) | async-done | bytes 131088 | tf_op jit(solution)/shard_map/psum | solution.py:156
  193.6 1.2 fusion.12
  194.8 16.0 %psum.63 = f32[16,256]{1,0:T(8,128)S(1)} all-reduce(f32[16,256]{1,0:T(8,128)S(1)} %fusion.12), channel_id=1, replica_groups=mesh['kv'=8,'tp'=4] {'tp'}, use_global_device_ids=true, to_apply=%region_18.19 | all-reduce | flops 4096 | bytes 32768 | tf_op jit(solution)/shard_map/psum | solution.py:160
  210.7 0.6 add_convert_fusion.1
  (78 shorter events, 3.2 us)
Async XLA Ops:
  7.2 38.4 %copy-start = (bf16[512,16,64]{0,2,1:T(8,128)(2,1)S(1)}, bf16[512,16,64]{0,2,1:T(8,128)(2,1)}, u32[]{:S(2)}) copy-start(bf16[512,16,64]{0,2,1:T(8,128)(2,1)} %param.29) | copy-start | bytes 3145732
  7.2 37.9 %copy-start.4 = (bf16[512,16,32]{0,2,1:T(8,128)(2,1)S(1)}, bf16[512,16,32]{0,2,1:T(8,128)(2,1)}, u32[]{:S(2)}) copy-start(bf16[512,16,32]{0,2,1:T(8,128)(2,1)} %param.30) | copy-start | bytes 1572868
  12.8 32.8 %copy-start.5 = (bf16[256,16,64]{0,2,1:T(8,128)(2,1)S(1)}, bf16[256,16,64]{0,2,1:T(8,128)(2,1)}, u32[]{:S(2)}) copy-start(bf16[256,16,64]{0,2,1:T(8,128)(2,1)} %param.32) | copy-start | bytes 1572868
  45.6 0.9 copy-start.8
  46.3 1.2 copy-start.1
  48.5 9.1 %all-to-all-start = ((f32[1,16,16]{1,0,2:T(1,128)}), f32[1,16,16]{1,0,2:T(1,128)S(1)}, u32[]{:S(2)}, u32[]{:S(2)}) async-start(f32[1,16,16]{1,0,2:T(1,128)} %copy.50), calls=%async_computation | async-start | bytes 16384 | tf_op jit(solution)/shard_map/all_to_all | solution.py:135
  52.2 0.7 copy-start.10
  54.3 0.6 copy-start.9
  55.3 0.7 copy-start.11
  57.6 17.0 %all-to-all-start.1 = ((f32[1,16,16]{1,0,2:T(1,128)}), f32[1,16,16]{1,0,2:T(1,128)S(1)}, u32[]{:S(2)}, u32[]{:S(2)}) async-start(f32[1,16,16]{1,0,2:T(1,128)} %copy.51), calls=%async_computation.1 | async-start | bytes 16384 | tf_op jit(solution)/shard_map/all_to_all | solution.py:136
  74.6 17.0 %all-to-all-start.2 = ((f32[1,16,16,256]{3,1,0,2:T(8,128)}), f32[1,16,16,256]{3,1,0,2:T(8,128)S(1)}, u32[]{:S(2)}, u32[]{:S(2)}) async-start(f32[1,16,16,256]{3,1,0,2:T(8,128)} %copy.52), calls=%async_computation.2 | async-start | bytes 524288 | tf_op jit(solution)/shard_map/all_to_all | solution.py:137
  78.8 114.8 %all-reduce.3.cloned.1.call-start = ((), (), s32[]{:S(2)}) async-start(), calls=%async_computation.3 | async-start | bytes 262144 | tf_op jit(solution)/shard_map/psum | solution.py:156
  91.7 19.0 %copy-start.7 = (bf16[4,64,256]{2,1,0:T(8,128)(2,1)S(1)}, bf16[4,64,256]{2,1,0:T(8,128)(2,1)}, u32[]{:S(2)}) copy-start(bf16[4,64,256]{2,1,0:T(8,128)(2,1)} %param.34) | copy-start | bytes 393220
  106.8 34.4 %copy-start.2 = (bf16[256,2048]{1,0:T(8,128)(2,1)S(1)}, bf16[256,2048]{1,0:T(8,128)(2,1)}, u32[]{:S(2)}) copy-start(bf16[256,2048]{1,0:T(8,128)(2,1)} %param.36) | copy-start | bytes 3145732
  106.8 20.7 %copy-start.6 = (bf16[16,256]{1,0:T(8,128)(2,1)S(1)}, bf16[16,256]{1,0:T(8,128)(2,1)}, u32[]{:S(2)}) copy-start(bf16[16,256]{1,0:T(8,128)(2,1)} %param.20) | copy-start | bytes 24580
  109.3 84.3 %copy-start.3 = (bf16[2048,256]{1,0:T(8,128)(2,1)S(1)}, bf16[2048,256]{1,0:T(8,128)(2,1)}, u32[]{:S(2)}) copy-start(bf16[2048,256]{1,0:T(8,128)(2,1)} %param.37) | copy-start | bytes 3145732
Sparse Core Ops, SparseCore 0:
  142.3 51.2 all-reduce.2
where the time goes:
time: 219 us; the launch traced here: 218 us
  blocking collectives  117 us (53%)
  waiting for transfers between devices  51.5 us (24%)
  between operations  14.2 us (6%)
  starting transfers between devices  12.1 us (6%)
  matrix products  8.74 us (4%)
  other arithmetic  7.81 us (4%)
  local copies, waits for them, and re-layouts  6.26 us (3%)
    psum x1, waiting for transfers between devices, per_device(): hidden_sum, total_mid = lax.psum((hidden_part, square_mid), 'kv')  51.4 us
    all_gather x3, blocking collectives, combined_all(): gathered = jax.tree.map(lambda a: lax.all_gather(a, axis), part)  40.6 us
    psum x1, blocking collectives, per_device(): lax.psum((part_q, part_kv, part_rope, square_in), 'kv')  30.8 us
    psum x1, blocking collectives, per_device(): resid_mid = resid + lax.psum(attn_part, 'tp')  16.5 us
    psum x1, blocking collectives, per_device(): mixed = (resid_mid + lax.psum(out_part, 'tp')).astype(bf16)  16 us
    psum x1, blocking collectives, per_device(): hidden_sum, total_mid = lax.psum((hidden_part, square_mid), 'kv')  13.6 us
  transfers between devices with their start and end apart: 4, of which 1 were waited for; matrix products, arithmetic and copies ran while one was open for 2% of the time, Pallas kernels for 0%

commit v1 on v0

v1 whole, which is shorter than its diff:
```python
import jax
import jax.numpy as jnp
from jax import lax
from jax.sharding import PartitionSpec as P

D = 2048
NOPE = 64
ROPE = 32
EPS = 1e-06


def swap(value, axis, bit):
    size = lax.axis_size(axis)
    return lax.ppermute(value, axis, [(j, j ^ bit) for j in range(size)])


def bits(axis):
    size = lax.axis_size(axis)
    found = [1 << i for i in range(size.bit_length() - 1)]
    assert 1 << len(found) == size
    return found


def summed(value, axis, skip=()):
    for bit in bits(axis):
        if bit not in skip:
            value = value + swap(value, axis, bit)
    return value


def my_half(value, dim, axis, bit):
    half = value.shape[dim] // 2
    mine = (lax.axis_index(axis) & bit) // bit
    keep = lax.dynamic_slice_in_dim(value, mine * half, half, dim)
    give = lax.dynamic_slice_in_dim(value, (1 - mine) * half, half, dim)
    return keep, give


def rotate(values, positions):
    half = values.shape[-1] // 2
    inverse = 10000.0 ** (-jnp.arange(half, dtype=jnp.float32) / half)
    angle = positions.astype(jnp.float32)[:, None, None] * inverse[None, None, :]
    first = values[..., :half]
    second = values[..., half:]
    return jnp.concatenate(
        [
            first * jnp.cos(angle) - second * jnp.sin(angle),
            second * jnp.cos(angle) + first * jnp.sin(angle),
        ],
        axis=-1,
    )


def rms_scaled(values, gain):
    return (
        values
        * lax.rsqrt(jnp.mean(values * values, axis=-1, keepdims=True) + EPS)
        * gain.astype(jnp.float32)
    )


def merged(one, two):
    top_one, top_two = one[..., -1:], two[..., -1:]
    top = jnp.maximum(top_one, top_two)
    body = one[..., :-1] * jnp.exp(top_one - top) + two[..., :-1] * jnp.exp(top_two - top)
    return jnp.concatenate([body, top], axis=-1)


def per_device(
    tokens,
    lengths,
    latent_cache,
    rope_cache,
    gain_in,
    w_down_q,
    w_down_kv,
    w_rope_key,
    gain_q,
    w_up_qn,
    w_up_qr,
    gain_kv,
    w_key_up,
    w_value_up,
    w_attn_out,
    gain_mid,
    w_ff_in,
    w_ff_out,
):
    f32 = jnp.float32
    bf16 = jnp.bfloat16
    scale = (NOPE + ROPE) ** (-0.5)
    resid = tokens.astype(f32)
    scaled_in = (resid * gain_in.astype(f32)).astype(bf16)
    part_q = jnp.dot(scaled_in, w_down_q, preferred_element_type=f32)
    part_kv = jnp.dot(scaled_in, w_down_kv, preferred_element_type=f32)
    part_rope = jnp.dot(scaled_in, w_rope_key, preferred_element_type=f32)
    square_in = jnp.sum(resid * resid, axis=1, keepdims=True)
    sums = summed(jnp.concatenate([part_q, part_kv, part_rope, square_in], axis=1), "kv")
    ends = [w_down_q.shape[1], w_down_q.shape[1] + w_down_kv.shape[1]]
    ends.append(ends[1] + w_rope_key.shape[1])
    sum_q, sum_kv, sum_rope, total_in = jnp.split(sums, ends, axis=1)
    inv_in = lax.rsqrt(total_in / D + EPS)
    query_latent = rms_scaled(inv_in * sum_q, gain_q).astype(bf16)
    new_latent = rms_scaled(inv_in * sum_kv, gain_kv).astype(bf16)
    new_rope_key = rotate((inv_in * sum_rope)[:, None, :], lengths)[:, 0, :].astype(bf16)
    query_nope = jnp.einsum(
        "bc,chd->bhd", query_latent, w_up_qn, preferred_element_type=f32
    ).astype(bf16)
    query_rope = rotate(
        jnp.einsum("bc,chr->bhr", query_latent, w_up_qr, preferred_element_type=f32), lengths
    ).astype(bf16)
    query_cache = jnp.einsum(
        "bhd,khd->bhk", query_nope, w_key_up, preferred_element_type=f32
    ).astype(bf16)
    rows = latent_cache.shape[1]
    positions = lax.axis_index(("kv", "tp")) * rows + jnp.arange(rows, dtype=jnp.int32)
    live = (positions[None, :] < lengths[:, None])[:, None, :]
    scores = (
        jnp.einsum("bhk,blk->bhl", query_cache, latent_cache, preferred_element_type=f32)
        + jnp.einsum("bhr,blr->bhl", query_rope, rope_cache, preferred_element_type=f32)
    ) * scale
    scores = jnp.where(live, scores, -1e30)
    top = jnp.max(scores, axis=2)
    weights = jnp.where(live, jnp.exp(scores - top[:, :, None]), 0.0)
    total = jnp.sum(weights, axis=2)
    acc = jnp.einsum("bhl,blk->bhk", weights.astype(bf16), latent_cache, preferred_element_type=f32)
    expanded = jnp.einsum(
        "bhk,khv->hbv", acc, w_value_up.astype(f32), precision=lax.Precision.HIGHEST
    )
    part = jnp.concatenate([expanded, total.T[:, :, None], top.T[:, :, None]], axis=2)
    for bit in reversed(bits("tp")):
        keep, give = my_half(part, 0, "tp", bit)
        part = merged(keep, swap(give, "tp", bit))
    for bit in bits("kv"):
        part = merged(part, swap(part, "kv", bit))
    heads_dev = w_attn_out.shape[0]
    first_head = lax.axis_index("tp") * heads_dev
    own_value_up = lax.dynamic_slice_in_dim(w_value_up, first_head, heads_dev, 1)
    own_cache_q = lax.dynamic_slice_in_dim(query_cache, first_head, heads_dev, 1)
    own_rope_q = lax.dynamic_slice_in_dim(query_rope, first_head, heads_dev, 1)
    self_score = (
        jnp.einsum("bhk,bk->hb", own_cache_q, new_latent, preferred_element_type=f32)
        + jnp.einsum("bhr,br->hb", own_rope_q, new_rope_key, preferred_element_type=f32)
    ) * scale
    self_value = jnp.einsum("bk,khv->hbv", new_latent, own_value_up, preferred_element_type=f32)
    top, total, expanded = part[..., -1], part[..., -2], part[..., :-2]
    joined = jnp.maximum(top, self_score)
    fade = jnp.exp(top - joined)
    self_weight = jnp.exp(self_score - joined)
    total = total * fade + self_weight
    expanded = (
        expanded * fade[..., None] + self_weight.astype(bf16).astype(f32)[..., None] * self_value
    )
    head_out = (expanded / total[..., None]).astype(bf16)
    attn_part = jnp.einsum("hbv,hvd->bd", head_out, w_attn_out, preferred_element_type=f32)
    resid_mid = resid + summed(attn_part, "tp")
    scaled_mid = (resid_mid * gain_mid.astype(f32)).astype(bf16)
    hidden_part = jnp.dot(scaled_mid, w_ff_in, preferred_element_type=f32)
    square_mid = jnp.sum(resid_mid * resid_mid, axis=1, keepdims=True)
    keep, give = my_half(hidden_part, 1, "kv", 1)
    keep = jnp.concatenate([keep, square_mid], axis=1)
    give = jnp.concatenate([give, square_mid], axis=1)
    sums = summed(keep + swap(give, "kv", 1), "kv", skip=(1,))
    other = swap(sums, "kv", 1)
    low = (lax.axis_index("kv") & 1) == 0
    inv_mid = lax.rsqrt(sums[:, -1:] / D + EPS)
    sums = jnp.concatenate(
        [jnp.where(low, sums, other)[:, :-1], jnp.where(low, other, sums)[:, :-1]], axis=1
    )
    hidden = jnp.square(jax.nn.relu(inv_mid * sums)).astype(bf16)
    out_part = jnp.dot(hidden, w_ff_out, preferred_element_type=f32)
    mixed = (resid_mid + summed(out_part, "tp")).astype(bf16)
    return (mixed, new_latent, new_rope_key)


def solution(mesh):
    return jax.shard_map(
        per_device,
        mesh=mesh,
        in_specs=(
            P(None, "kv"),
            P(),
            P(None, ("kv", "tp"), None),
            P(None, ("kv", "tp"), None),
            P("kv"),
            P("kv", None),
            P("kv", None),
            P("kv", None),
            P(),
            P(),
            P(),
            P(),
            P(),
            P(),
            P("tp", None, "kv"),
            P("kv"),
            P("kv", "tp"),
            P("tp", "kv"),
        ),
        out_specs=(P(None, "kv"), P(), P()),
        check_vma=False,
    )
```

time: 219 us -> 73.3 us (0.33)
  blocking collectives: 117 us -> 0 us
  waiting for transfers between devices: 51.5 us -> 29.1 us
  starting transfers between devices: 12.1 us -> 26.6 us
  between operations: 14.2 us -> 1.02 us
  local copies, waits for them, and re-layouts: 6.26 us -> 3.35 us
    psum x4 -> x0, blocking collectives: 76.9 us -> none  [the longest x1 30.8 us: per_device(): lax.psum((part_q, part_kv, part_rope, square_in), 'kv')]
    psum x1 -> x0, waiting for transfers between devices: 51.4 us -> none  [per_device(): hidden_sum, total_mid = lax.psum((hidden_part, square_mid), 'kv')]
    all_gather x3 -> x0, blocking collectives: 40.6 us -> none  [combined_all(): gathered = jax.tree.map(lambda a: lax.all_gather(a, axis), part)]
    ppermute x0 -> x16, waiting for transfers between devices: none -> 29.1 us  [swap(): return lax.ppermute(value, axis, [(j, j ^ bit) for j in range(size)])]
    ppermute x0 -> x16, starting transfers between devices: none -> 26.6 us  [swap(): return lax.ppermute(value, axis, [(j, j ^ bit) for j in range(size)])]
    all_to_all x3 -> x0, starting transfers between devices: 12.1 us -> none  [the longest x1 4.19 us: per_device(): lax.all_to_all(total[None], 'tp', split_axis=2, concat_axis=0, tiled=True)]
  transfers between devices with their start and end apart: 4 -> 16, of which waited for: 1 -> 16; matrix products, arithmetic and copies ran while one was open for 2% -> 2% of each run, Pallas kernels for 0% -> 0%
where the time goes in v1:
time: 73.3 us; the launch traced here: 72.9 us
  waiting for transfers between devices  29.1 us (40%)
  starting transfers between devices  26.6 us (36%)
  matrix products  6.77 us (9%)
  other arithmetic  6.11 us (8%)
  local copies, waits for them, and re-layouts  3.35 us (5%)
  between operations  1.02 us (1%)
    ppermute x16, waiting for transfers between devices, swap(): return lax.ppermute(value, axis, [(j, j ^ bit) for j in range(size)])  29.1 us
    ppermute x16, starting transfers between devices, swap(): return lax.ppermute(value, axis, [(j, j ^ bit) for j in range(size)])  26.6 us
    unnamed x32, local copies, waits for them, and re-layouts  2.48 us
  transfers between devices with their start and end apart: 16, of which 16 were waited for; matrix products, arithmetic and copies ran while one was open for 2% of the time, Pallas kernels for 0%

profile of v1, /device:TPU:0, one launch (start us, length us, event | category | flops | bytes accessed | tf_op | source)
XLA Modules:
  0.0 72.9 jit_solution(1216889161352415803)
XLA Ops:
  0.7 0.9 %fusion.37 = f32[16]{0:T(128)S(1)} fusion(bf16[16,256]{1,0:T(8,128)(2,1)} %param.18), kind=kLoop, calls=%fused_computation.91 | loop fusion | flops 12272 | bytes 8256 | tf_op jit(solution)/shard_map/reduce_sum | solution.py:97
  1.7 0.6 copy-done.7
  2.3 0.8 %fusion.70 = f32[16,32]{1,0:T(8,128)S(1)} fusion(bf16[256,32]{0,1:T(8,128)(2,1)} %param.25, bf16[16,256]{1,0:T(8,128)(2,1)S(1)} %copy-done.7, f32[256]{0:T(256)S(1)} %convert_element_type.65), kind=kOutput, calls=%fused_computation.132 | convolution fusion | flops 274432 | bytes 27648 | tf_op jit(solution)/shard_map/dot_general | solution.py:96
  3.1 1.1 %fusion.72 = f32[16,256]{1,0:T(8,128)S(1)} fusion(bf16[256,256]{1,0:T(8,128)(2,1)} %param.24, bf16[16,256]{1,0:T(8,128)(2,1)S(1)} %copy-done.7, f32[256]{0:T(256)S(1)} %convert_element_type.65), kind=kOutput, calls=%fused_computation.133 | convolution fusion | flops 2109440 | bytes 156672 | tf_op jit(solution)/shard_map/dot_general | solution.py:95
  4.2 1.2 %fusion.74 = f32[16,512]{1,0:T(8,128)S(1)} fusion(bf16[256,512]{1,0:T(8,128)(2,1)} %param.23, bf16[16,256]{1,0:T(8,128)(2,1)S(1)} %copy-done.7, f32[256]{0:T(256)S(1)} %convert_element_type.65), kind=kOutput, calls=%fused_computation.134 | convolution fusion | flops 4206592 | bytes 304128 | tf_op jit(solution)/shard_map/dot_general | solution.py:94
  5.4 0.5 collective-permute-start
  6.1 0.7 %collective-permute-done = f32[16,801]{1,0:T(8,128)S(1)} collective-permute-done((f32[16,801]{1,0:T(8,128)S(1)}, f32[16,801]{1,0:T(8,128)S(1)}, u32[]{:S(2)}, u32[]{:S(2)}) %collective-permute-start) | collective-permute-done | bytes 51296 | tf_op jit(solution)/shard_map/ppermute | solution.py:14
  6.9 2.9 %collective-permute-start.1 = (f32[16,801]{1,0:T(8,128)S(1)}, f32[16,801]{1,0:T(8,128)S(1)}, u32[]{:S(2)}, u32[]{:S(2)}) collective-permute-start(f32[16,801]{1,0:T(8,128)S(1)} %fusion.108), channel_id=1, source_target_pairs={{0,8},{4,12},{8,0},{12,4},{16,24},{20,28},{24,16},{28,20},{1,9},{5... | collective-permute-start | bytes 153800 | tf_op jit(solution)/shard_map/ppermute | solution.py:14
  9.8 2.2 %collective-permute-done.1 = f32[16,801]{1,0:T(8,128)S(1)} collective-permute-done((f32[16,801]{1,0:T(8,128)S(1)}, f32[16,801]{1,0:T(8,128)S(1)}, u32[]{:S(2)}, u32[]{:S(2)}) %collective-permute-start.1) | collective-permute-done | bytes 51296 | tf_op jit(solution)/shard_map/ppermute | solution.py:14
  12.1 3.0 %collective-permute-start.2 = (f32[16,801]{1,0:T(8,128)S(1)}, f32[16,801]{1,0:T(8,128)S(1)}, u32[]{:S(2)}, u32[]{:S(2)}) collective-permute-start(f32[16,801]{1,0:T(8,128)S(1)} %add.135), channel_id=1, source_target_pairs={{0,16},{4,20},{8,24},{12,28},{16,0},{20,4},{24,8},{28,12},{1,17},{... | collective-permute-start | bytes 153800 | tf_op jit(solution)/shard_map/ppermute | solution.py:14
  15.2 2.0 %collective-permute-done.2 = f32[16,801]{1,0:T(8,128)S(1)} collective-permute-done((f32[16,801]{1,0:T(8,128)S(1)}, f32[16,801]{1,0:T(8,128)S(1)}, u32[]{:S(2)}, u32[]{:S(2)}) %collective-permute-start.2) | collective-permute-done | bytes 51296 | tf_op jit(solution)/shard_map/ppermute | solution.py:14
  17.9 0.5 fusion.88
  18.4 0.7 convolution_convert_fusion
  19.5 0.8 %copy-done.1 = bf16[16,96,256]{2,1,0:T(8,128)(2,1)S(1)} copy-done((bf16[16,96,256]{2,1,0:T(8,128)(2,1)S(1)}, bf16[16,96,256]{2,1,0:T(8,128)(2,1)}, u32[]{:S(2)}) %copy-start.1) | copy-done | bytes 786456
  20.2 0.4 fusion.93
  20.6 0.2 fusion.10
  20.8 0.3 fusion.13
  21.5 0.4 copy-done.4
  21.9 0.6 fusion.3
  22.6 1.9 %collective-permute-start.3 = (f32[8,16,66]{2,1,0:T(8,128)S(1)}, f32[8,16,66]{2,1,0:T(8,128)S(1)}, u32[]{:S(2)}, u32[]{:S(2)}) collective-permute-start(f32[8,16,66]{2,1,0:T(8,128)S(1)} %constant_dynamic-slice_fusion.2), channel_id=1, source_target_pairs={{0,2},{1,3},{2,0},{3,1},{4,6},{5,7},{6,4},{7,5},{8,10},{9,11},{10,... | collective-permute-start | bytes 101384 | tf_op jit(solution)/shard_map/ppermute | solution.py:14
  24.9 2.1 %collective-permute-done.3 = f32[8,16,66]{2,1,0:T(8,128)S(1)} collective-permute-done((f32[8,16,66]{2,1,0:T(8,128)S(1)}, f32[8,16,66]{2,1,0:T(8,128)S(1)}, u32[]{:S(2)}, u32[]{:S(2)}) %collective-permute-start.3) | collective-permute-done | bytes 33824 | tf_op jit(solution)/shard_map/ppermute | solution.py:14
  27.4 1.9 %collective-permute-start.4 = (f32[4,16,66]{2,1,0:T(8,128)S(1)}, f32[4,16,66]{2,1,0:T(8,128)S(1)}, u32[]{:S(2)}, u32[]{:S(2)}) collective-permute-start(f32[4,16,66]{2,1,0:T(8,128)S(1)} %get-tuple-element.28), channel_id=1, source_target_pairs={{0,1},{1,0},{2,3},{3,2},{4,5},{5,4},{6,7},{7,6},{8,9},{9,8},{10,11... | collective-permute-start | bytes 50696 | tf_op jit(solution)/shard_map/ppermute | solution.py:14
  29.4 2.0 %collective-permute-done.4 = f32[4,16,66]{2,1,0:T(8,128)S(1)} collective-permute-done((f32[4,16,66]{2,1,0:T(8,128)S(1)}, f32[4,16,66]{2,1,0:T(8,128)S(1)}, u32[]{:S(2)}, u32[]{:S(2)}) %collective-permute-start.4) | collective-permute-done | bytes 16928 | tf_op jit(solution)/shard_map/ppermute | solution.py:14
  31.8 0.7 fusion.82
  32.4 0.5 collective-permute-done.5
  33.3 1.9 %collective-permute-start.6 = (f32[4,16,66]{2,1,0:T(8,128)S(1)}, f32[4,16,66]{2,1,0:T(8,128)S(1)}, u32[]{:S(2)}, u32[]{:S(2)}) collective-permute-start(f32[4,16,66]{2,1,0:T(8,128)S(1)} %pad_maximum_fusion.6), channel_id=1, source_target_pairs={{0,8},{4,12},{8,0},{12,4},{16,24},{20,28},{24,16},{28,20},{1,9},{5... | collective-permute-start | bytes 50696 | tf_op jit(solution)/shard_map/ppermute | solution.py:14
  35.4 1.9 %collective-permute-done.6 = f32[4,16,66]{2,1,0:T(8,128)S(1)} collective-permute-done((f32[4,16,66]{2,1,0:T(8,128)S(1)}, f32[4,16,66]{2,1,0:T(8,128)S(1)}, u32[]{:S(2)}, u32[]{:S(2)}) %collective-permute-start.6) | collective-permute-done | bytes 16928 | tf_op jit(solution)/shard_map/ppermute | solution.py:14
  37.6 3.0 %collective-permute-start.7 = (f32[4,16,66]{2,1,0:T(8,128)S(1)}, f32[4,16,66]{2,1,0:T(8,128)S(1)}, u32[]{:S(2)}, u32[]{:S(2)}) collective-permute-start(f32[4,16,66]{2,1,0:T(8,128)S(1)} %pad_maximum_fusion.7), channel_id=1, source_target_pairs={{0,16},{4,20},{8,24},{12,28},{16,0},{20,4},{24,8},{28,12},{1,17},{... | collective-permute-start | bytes 50696 | tf_op jit(solution)/shard_map/ppermute | solution.py:14
  40.8 1.8 %collective-permute-done.7 = f32[4,16,66]{2,1,0:T(8,128)S(1)} collective-permute-done((f32[4,16,66]{2,1,0:T(8,128)S(1)}, f32[4,16,66]{2,1,0:T(8,128)S(1)}, u32[]{:S(2)}, u32[]{:S(2)}) %collective-permute-start.7) | collective-permute-done | bytes 16928 | tf_op jit(solution)/shard_map/ppermute | solution.py:14
  43.1 0.4 convolution_bitcast_fusion
  43.4 1.6 %collective-permute-start.8 = (f32[16,256]{1,0:T(8,128)S(1)}, f32[16,256]{1,0:T(8,128)S(1)}, u32[]{:S(2)}, u32[]{:S(2)}) collective-permute-start(f32[16,256]{1,0:T(8,128)S(1)} %convolution_bitcast_fusion), channel_id=1, source_target_pairs={{0,1},{1,0},{2,3},{3,2},{4,5},{5,4},{6,7},{7,6},{8,9},{9,8},{10,11... | collective-permute-start | bytes 49160 | tf_op jit(solution)/shard_map/ppermute | solution.py:14
  45.1 2.1 %collective-permute-done.8 = f32[16,256]{1,0:T(8,128)S(1)} collective-permute-done((f32[16,256]{1,0:T(8,128)S(1)}, f32[16,256]{1,0:T(8,128)S(1)}, u32[]{:S(2)}, u32[]{:S(2)}) %collective-permute-start.8) | collective-permute-done | bytes 16416 | tf_op jit(solution)/shard_map/ppermute | solution.py:14
  47.2 1.7 %collective-permute-start.9 = (f32[16,256]{1,0:T(8,128)S(1)}, f32[16,256]{1,0:T(8,128)S(1)}, u32[]{:S(2)}, u32[]{:S(2)}) collective-permute-start(f32[16,256]{1,0:T(8,128)S(1)} %add.156), channel_id=1, source_target_pairs={{0,2},{1,3},{2,0},{3,1},{4,6},{5,7},{6,4},{7,5},{8,10},{9,11},{10,... | collective-permute-start | bytes 49160 | tf_op jit(solution)/shard_map/ppermute | solution.py:14
  48.9 0.7 copy-done.15
  49.5 1.4 %collective-permute-done.9 = f32[16,256]{1,0:T(8,128)S(1)} collective-permute-done((f32[16,256]{1,0:T(8,128)S(1)}, f32[16,256]{1,0:T(8,128)S(1)}, u32[]{:S(2)}, u32[]{:S(2)}) %collective-permute-start.9) | collective-permute-done | bytes 16416 | tf_op jit(solution)/shard_map/ppermute | solution.py:14
  51.1 0.3 fusion.60
  51.5 1.3 %collective-permute-done.10 = f32[16,1025]{1,0:T(8,128)S(1)} collective-permute-done((f32[16,1025]{1,0:T(8,128)S(1)}, f32[16,1025]{1,0:T(8,128)S(1)}, u32[]{:S(2)}, u32[]{:S(2)}) %collective-permute-start.10) | collective-permute-done | bytes 65632 | tf_op jit(solution)/shard_map/ppermute | solution.py:14
  52.8 2.0 %collective-permute-start.11 = (f32[16,1025]{1,0:T(8,128)S(1)}, f32[16,1025]{1,0:T(8,128)S(1)}, u32[]{:S(2)}, u32[]{:S(2)}) collective-permute-start(f32[16,1025]{1,0:T(8,128)S(1)} %fusion.12), channel_id=1, source_target_pairs={{0,8},{4,12},{8,0},{12,4},{16,24},{20,28},{24,16},{28,20},{1,9},{5... | collective-permute-start | bytes 196808 | tf_op jit(solution)/shard_map/ppermute | solution.py:14
  54.7 2.6 %collective-permute-done.11 = f32[16,1025]{1,0:T(8,128)S(1)} collective-permute-done((f32[16,1025]{1,0:T(8,128)S(1)}, f32[16,1025]{1,0:T(8,128)S(1)}, u32[]{:S(2)}, u32[]{:S(2)}) %collective-permute-start.11) | collective-permute-done | bytes 65632 | tf_op jit(solution)/shard_map/ppermute | solution.py:14
  57.3 3.0 %collective-permute-start.12 = (f32[16,1025]{1,0:T(8,128)S(1)}, f32[16,1025]{1,0:T(8,128)S(1)}, u32[]{:S(2)}, u32[]{:S(2)}) collective-permute-start(f32[16,1025]{1,0:T(8,128)S(1)} %add.162), channel_id=1, source_target_pairs={{0,16},{4,20},{8,24},{12,28},{16,0},{20,4},{24,8},{28,12},{1,17},{... | collective-permute-start | bytes 196808 | tf_op jit(solution)/shard_map/ppermute | solution.py:14
  60.3 2.8 %collective-permute-done.12 = f32[16,1025]{1,0:T(8,128)S(1)} collective-permute-done((f32[16,1025]{1,0:T(8,128)S(1)}, f32[16,1025]{1,0:T(8,128)S(1)}, u32[]{:S(2)}, u32[]{:S(2)}) %collective-permute-start.12) | collective-permute-done | bytes 65632 | tf_op jit(solution)/shard_map/ppermute | solution.py:14
  63.3 1.1 %collective-permute-done.13 = f32[16,1025]{1,0:T(8,128)S(1)} collective-permute-done((f32[16,1025]{1,0:T(8,128)S(1)}, f32[16,1025]{1,0:T(8,128)S(1)}, u32[]{:S(2)}, u32[]{:S(2)}) %collective-permute-start.13) | collective-permute-done | bytes 65632 | tf_op jit(solution)/shard_map/ppermute | solution.py:14
  64.5 0.3 fusion.15
  64.8 1.5 %collective-permute-start.14 = (f32[16,256]{1,0:T(8,128)S(1)}, f32[16,256]{1,0:T(8,128)S(1)}, u32[]{:S(2)}, u32[]{:S(2)}) collective-permute-start(f32[16,256]{1,0:T(8,128)S(1)} %fusion.15), channel_id=1, source_target_pairs={{0,1},{1,0},{2,3},{3,2},{4,5},{5,4},{6,7},{7,6},{8,9},{9,8},{10,11... | collective-permute-start | bytes 49160 | tf_op jit(solution)/shard_map/ppermute | solution.py:14
  66.3 2.2 %collective-permute-done.14 = f32[16,256]{1,0:T(8,128)S(1)} collective-permute-done((f32[16,256]{1,0:T(8,128)S(1)}, f32[16,256]{1,0:T(8,128)S(1)}, u32[]{:S(2)}, u32[]{:S(2)}) %collective-permute-start.14) | collective-permute-done | bytes 16416 | tf_op jit(solution)/shard_map/ppermute | solution.py:14
  68.5 1.5 %collective-permute-start.15 = (f32[16,256]{1,0:T(8,128)S(1)}, f32[16,256]{1,0:T(8,128)S(1)}, u32[]{:S(2)}, u32[]{:S(2)}) collective-permute-start(f32[16,256]{1,0:T(8,128)S(1)} %add.165), channel_id=1, source_target_pairs={{0,2},{1,3},{2,0},{3,1},{4,6},{5,7},{6,4},{7,5},{8,10},{9,11},{10,... | collective-permute-start | bytes 49160 | tf_op jit(solution)/shard_map/ppermute | solution.py:14
  70.1 2.2 %collective-permute-done.15 = f32[16,256]{1,0:T(8,128)S(1)} collective-permute-done((f32[16,256]{1,0:T(8,128)S(1)}, f32[16,256]{1,0:T(8,128)S(1)}, u32[]{:S(2)}, u32[]{:S(2)}) %collective-permute-start.15) | collective-permute-done | bytes 16416 | tf_op jit(solution)/shard_map/ppermute | solution.py:14
  72.3 0.6 add_convert_fusion.1
  (94 shorter events, 5.3 us)
Async XLA Ops:
  0.6 17.7 %copy-start = (bf16[512,16,64]{0,2,1:T(8,128)(2,1)S(1)}, bf16[512,16,64]{0,2,1:T(8,128)(2,1)}, u32[]{:S(2)}) copy-start(bf16[512,16,64]{0,2,1:T(8,128)(2,1)} %param.27) | copy-start | bytes 3145732
  0.6 0.9 %copy-start.13 = (bf16[256]{0:T(256)(128)(2,1)S(1)}, bf16[256]{0:T(256)(128)(2,1)}, u32[]{:S(2)}) copy-start(bf16[256]{0:T(256)(128)(2,1)} %param.22) | copy-start | bytes 1540
  1.6 0.7 copy-start.7
  3.1 2.8 %copy-start.11 = (s32[16]{0:T(128)S(1)}, s32[16]{0:T(128)}, u32[]{:S(2)}) copy-start(s32[16]{0:T(128)} %param.19) | copy-start | bytes 196
  4.2 13.7 %copy-start.5 = (bf16[512,16,32]{0,2,1:T(8,128)(2,1)S(1)}, bf16[512,16,32]{0,2,1:T(8,128)(2,1)}, u32[]{:S(2)}) copy-start(bf16[512,16,32]{0,2,1:T(8,128)(2,1)} %param.28) | copy-start | bytes 1572868
  5.4 1.4 %collective-permute-start = (f32[16,801]{1,0:T(8,128)S(1)}, f32[16,801]{1,0:T(8,128)S(1)}, u32[]{:S(2)}, u32[]{:S(2)}) collective-permute-start(f32[16,801]{1,0:T(8,128)S(1)} %pad_maximum_fusion.4), channel_id=1, source_target_pairs={{0,4},{4,0},{8,12},{12,8},{16,20},{20,16},{24,28},{28,24},{1,5},{5... | collective-permute-start | bytes 153800 | tf_op jit(solution)/shard_map/ppermute | solution.py:14
  6.9 5.2 %collective-permute-start.1 = (f32[16,801]{1,0:T(8,128)S(1)}, f32[16,801]{1,0:T(8,128)S(1)}, u32[]{:S(2)}, u32[]{:S(2)}) collective-permute-start(f32[16,801]{1,0:T(8,128)S(1)} %fusion.108), channel_id=1, source_target_pairs={{0,8},{4,12},{8,0},{12,4},{16,24},{20,28},{24,16},{28,20},{1,9},{5... | collective-permute-start | bytes 153800 | tf_op jit(solution)/shard_map/ppermute | solution.py:14
  12.0 3.1 %copy-start.14 = (bf16[256]{0:T(256)(128)(2,1)S(1)}, bf16[256]{0:T(256)(128)(2,1)}, u32[]{:S(2)}) copy-start(bf16[256]{0:T(256)(128)(2,1)} %param.29) | copy-start | bytes 1540
  12.0 3.1 %copy-start.10 = (bf16[512]{0:T(512)(128)(2,1)S(1)}, bf16[512]{0:T(512)(128)(2,1)}, u32[]{:S(2)}) copy-start(bf16[512]{0:T(512)(128)(2,1)} %param.26) | copy-start | bytes 3076
  12.0 6.3 %copy-start.6 = (bf16[256,16,64]{0,2,1:T(8,128)(2,1)S(1)}, bf16[256,16,64]{0,2,1:T(8,128)(2,1)}, u32[]{:S(2)}) copy-start(bf16[256,16,64]{0,2,1:T(8,128)(2,1)} %param.30) | copy-start | bytes 1572868
  12.1 5.2 %collective-permute-start.2 = (f32[16,801]{1,0:T(8,128)S(1)}, f32[16,801]{1,0:T(8,128)S(1)}, u32[]{:S(2)}, u32[]{:S(2)}) collective-permute-start(f32[16,801]{1,0:T(8,128)S(1)} %add.135), channel_id=1, source_target_pairs={{0,16},{4,20},{8,24},{12,28},{16,0},{20,4},{24,8},{28,12},{1,17},{... | collective-permute-start | bytes 153800 | tf_op jit(solution)/shard_map/ppermute | solution.py:14
  18.4 0.9 %copy-start.8 = (bf16[16,96,32]{1,2,0:T(8,128)(2,1)S(1)}, bf16[16,96,32]{1,2,0:T(8,128)(2,1)}, u32[]{:S(2)}) copy-start(bf16[16,96,32]{1,2,0:T(8,128)(2,1)} %param.21) | copy-start | bytes 294916
  19.1 1.2 %copy-start.1 = (bf16[16,96,256]{2,1,0:T(8,128)(2,1)S(1)}, bf16[16,96,256]{2,1,0:T(8,128)(2,1)}, u32[]{:S(2)}) copy-start(bf16[16,96,256]{2,1,0:T(8,128)(2,1)} %param.20) | copy-start | bytes 2359300
  20.8 1.0 %copy-start.4 = (bf16[256,16,64]{0,2,1:T(8,128)(2,1)S(1)}, bf16[256,16,64]{0,2,1:T(8,128)(2,1)}, u32[]{:S(2)}) copy-start(bf16[256,16,64]{0,2,1:T(8,128)(2,1)} %param.31) | copy-start | bytes 1572868
  22.6 4.3 %collective-permute-start.3 = (f32[8,16,66]{2,1,0:T(8,128)S(1)}, f32[8,16,66]{2,1,0:T(8,128)S(1)}, u32[]{:S(2)}, u32[]{:S(2)}) collective-permute-start(f32[8,16,66]{2,1,0:T(8,128)S(1)} %constant_dynamic-slice_fusion.2), channel_id=1, source_target_pairs={{0,2},{1,3},{2,0},{3,1},{4,6},{5,7},{6,4},{7,5},{8,10},{9,11},{10,... | collective-permute-start | bytes 101384 | tf_op jit(solution)/shard_map/ppermute | solution.py:14
  27.3 23.8 %copy-start.2 = (bf16[256,2048]{1,0:T(8,128)(2,1)S(1)}, bf16[256,2048]{1,0:T(8,128)(2,1)}, u32[]{:S(2)}) copy-start(bf16[256,2048]{1,0:T(8,128)(2,1)} %param.34) | copy-start | bytes 3145732
  27.4 4.0 %collective-permute-start.4 = (f32[4,16,66]{2,1,0:T(8,128)S(1)}, f32[4,16,66]{2,1,0:T(8,128)S(1)}, u32[]{:S(2)}, u32[]{:S(2)}) collective-permute-start(f32[4,16,66]{2,1,0:T(8,128)S(1)} %get-tuple-element.28), channel_id=1, source_target_pairs={{0,1},{1,0},{2,3},{3,2},{4,5},{5,4},{6,7},{7,6},{8,9},{9,8},{10,11... | collective-permute-start | bytes 50696 | tf_op jit(solution)/shard_map/ppermute | solution.py:14
  31.7 1.2 %collective-permute-start.5 = (f32[4,16,66]{2,1,0:T(8,128)S(1)}, f32[4,16,66]{2,1,0:T(8,128)S(1)}, u32[]{:S(2)}, u32[]{:S(2)}) collective-permute-start(f32[4,16,66]{2,1,0:T(8,128)S(1)} %pad_maximum_fusion.5), channel_id=1, source_target_pairs={{0,4},{4,0},{8,12},{12,8},{16,20},{20,16},{24,28},{28,24},{1,5},{5... | collective-permute-start | bytes 50696 | tf_op jit(solution)/shard_map/ppermute | solution.py:14
  33.3 3.9 %collective-permute-start.6 = (f32[4,16,66]{2,1,0:T(8,128)S(1)}, f32[4,16,66]{2,1,0:T(8,128)S(1)}, u32[]{:S(2)}, u32[]{:S(2)}) collective-permute-start(f32[4,16,66]{2,1,0:T(8,128)S(1)} %pad_maximum_fusion.6), channel_id=1, source_target_pairs={{0,8},{4,12},{8,0},{12,4},{16,24},{20,28},{24,16},{28,20},{1,9},{5... | collective-permute-start | bytes 50696 | tf_op jit(solution)/shard_map/ppermute | solution.py:14
  37.6 5.0 %collective-permute-start.7 = (f32[4,16,66]{2,1,0:T(8,128)S(1)}, f32[4,16,66]{2,1,0:T(8,128)S(1)}, u32[]{:S(2)}, u32[]{:S(2)}) collective-permute-start(f32[4,16,66]{2,1,0:T(8,128)S(1)} %pad_maximum_fusion.7), channel_id=1, source_target_pairs={{0,16},{4,20},{8,24},{12,28},{16,0},{20,4},{24,8},{28,12},{1,17},{... | collective-permute-start | bytes 50696 | tf_op jit(solution)/shard_map/ppermute | solution.py:14
  40.7 2.4 %copy-start.9 = (bf16[16,256]{1,0:T(8,128)(2,1)}, bf16[16,256]{1,0:T(8,128)(2,1)S(1)}, u32[]{:S(2)}) copy-start(bf16[16,256]{1,0:T(8,128)(2,1)S(1)} %multiply_convert_fusion.2) | copy-start | bytes 24580
  40.7 2.4 %copy-start.12 = (bf16[4,64,256]{2,1,0:T(8,128)(2,1)S(1)}, bf16[4,64,256]{2,1,0:T(8,128)(2,1)}, u32[]{:S(2)}) copy-start(bf16[4,64,256]{2,1,0:T(8,128)(2,1)} %param.32) | copy-start | bytes 393220
  43.4 3.7 %collective-permute-start.8 = (f32[16,256]{1,0:T(8,128)S(1)}, f32[16,256]{1,0:T(8,128)S(1)}, u32[]{:S(2)}, u32[]{:S(2)}) collective-permute-start(f32[16,256]{1,0:T(8,128)S(1)} %convolution_bitcast_fusion), channel_id=1, source_target_pairs={{0,1},{1,0},{2,3},{3,2},{4,5},{5,4},{6,7},{7,6},{8,9},{9,8},{10,11... | collective-permute-start | bytes 49160 | tf_op jit(solution)/shard_map/ppermute | solution.py:14
  47.2 3.7 %collective-permute-start.9 = (f32[16,256]{1,0:T(8,128)S(1)}, f32[16,256]{1,0:T(8,128)S(1)}, u32[]{:S(2)}, u32[]{:S(2)}) collective-permute-start(f32[16,256]{1,0:T(8,128)S(1)} %add.156), channel_id=1, source_target_pairs={{0,2},{1,3},{2,0},{3,1},{4,6},{5,7},{6,4},{7,5},{8,10},{9,11},{10,... | collective-permute-start | bytes 49160 | tf_op jit(solution)/shard_map/ppermute | solution.py:14
  48.8 0.7 copy-start.15
  51.1 13.4 %copy-start.3 = (bf16[2048,256]{1,0:T(8,128)(2,1)S(1)}, bf16[2048,256]{1,0:T(8,128)(2,1)}, u32[]{:S(2)}) copy-start(bf16[2048,256]{1,0:T(8,128)(2,1)} %param.35) | copy-start | bytes 3145732
  51.4 1.3 %collective-permute-start.10 = (f32[16,1025]{1,0:T(8,128)S(1)}, f32[16,1025]{1,0:T(8,128)S(1)}, u32[]{:S(2)}, u32[]{:S(2)}) collective-permute-start(f32[16,1025]{1,0:T(8,128)S(1)} %pad_maximum_fusion.1), channel_id=1, source_target_pairs={{0,4},{4,0},{8,12},{12,8},{16,20},{20,16},{24,28},{28,24},{1,5},{5... | collective-permute-start | bytes 196808 | tf_op jit(solution)/shard_map/ppermute | solution.py:14
  52.8 4.5 %collective-permute-start.11 = (f32[16,1025]{1,0:T(8,128)S(1)}, f32[16,1025]{1,0:T(8,128)S(1)}, u32[]{:S(2)}, u32[]{:S(2)}) collective-permute-start(f32[16,1025]{1,0:T(8,128)S(1)} %fusion.12), channel_id=1, source_target_pairs={{0,8},{4,12},{8,0},{12,4},{16,24},{20,28},{24,16},{28,20},{1,9},{5... | collective-permute-start | bytes 196808 | tf_op jit(solution)/shard_map/ppermute | solution.py:14
  57.3 5.8 %collective-permute-start.12 = (f32[16,1025]{1,0:T(8,128)S(1)}, f32[16,1025]{1,0:T(8,128)S(1)}, u32[]{:S(2)}, u32[]{:S(2)}) collective-permute-start(f32[16,1025]{1,0:T(8,128)S(1)} %add.162), channel_id=1, source_target_pairs={{0,16},{4,20},{8,24},{12,28},{16,0},{20,4},{24,8},{28,12},{1,17},{... | collective-permute-start | bytes 196808 | tf_op jit(solution)/shard_map/ppermute | solution.py:14
  63.1 1.3 %collective-permute-start.13 = (f32[16,1025]{1,0:T(8,128)S(1)}, f32[16,1025]{1,0:T(8,128)S(1)}, u32[]{:S(2)}, u32[]{:S(2)}) collective-permute-start(f32[16,1025]{1,0:T(8,128)S(1)} %add.163), channel_id=1, source_target_pairs={{0,4},{4,0},{8,12},{12,8},{16,20},{20,16},{24,28},{28,24},{1,5},{5... | collective-permute-start | bytes 196808 | tf_op jit(solution)/shard_map/ppermute | solution.py:14
  64.8 3.7 %collective-permute-start.14 = (f32[16,256]{1,0:T(8,128)S(1)}, f32[16,256]{1,0:T(8,128)S(1)}, u32[]{:S(2)}, u32[]{:S(2)}) collective-permute-start(f32[16,256]{1,0:T(8,128)S(1)} %fusion.15), channel_id=1, source_target_pairs={{0,1},{1,0},{2,3},{3,2},{4,5},{5,4},{6,7},{7,6},{8,9},{9,8},{10,11... | collective-permute-start | bytes 49160 | tf_op jit(solution)/shard_map/ppermute | solution.py:14
  68.5 3.7 %collective-permute-start.15 = (f32[16,256]{1,0:T(8,128)S(1)}, f32[16,256]{1,0:T(8,128)S(1)}, u32[]{:S(2)}, u32[]{:S(2)}) collective-permute-start(f32[16,256]{1,0:T(8,128)S(1)} %add.165), channel_id=1, source_target_pairs={{0,2},{1,3},{2,0},{3,1},{4,6},{5,7},{6,4},{7,5},{8,10},{9,11},{10,... | collective-permute-start | bytes 49160 | tf_op jit(solution)/shard_map/ppermute | solution.py:14

commit v2 on v0

v2 whole, which is shorter than its diff:
```python
import functools

import jax
import jax.numpy as jnp
import numpy as np
from jax import lax
from jax.experimental import pallas as pl
from jax.experimental.pallas import tpu as pltpu
from jax.sharding import PartitionSpec as P

D = 2048
EPS = 1e-06
LANES = 128
MXU = 256
f32 = jnp.float32
bf16 = jnp.bfloat16
BOTH = ("kv", "tp")


def swap(value, kv_mask, tp_mask=0):
    n_kv, n_tp = lax.axis_size("kv"), lax.axis_size("tp")
    pairs = [
        (k * n_tp + t, (k ^ kv_mask) * n_tp + (t ^ tp_mask)) for k in range(n_kv) for t in range(n_tp)
    ]
    return lax.ppermute(value, BOTH, pairs)


def higher_bits(axis, first):
    size = lax.axis_size(axis)
    assert size & (size - 1) == 0
    return [1 << i for i in range(first, size.bit_length() - 1)]


def parity():
    ones = 0
    for axis in BOTH:
        index = lax.axis_index(axis)
        for i in range(lax.axis_size(axis).bit_length() - 1):
            ones = ones ^ ((index >> i) & 1)
    return ones


def call(kernel, outs, *args, scratch=(), far=()):
    near = pl.BlockSpec(memory_space=pltpu.VMEM)
    return pl.pallas_call(
        kernel,
        out_shape=[pltpu.VMEM(s, t) for s, t in outs],
        in_specs=[near] * len(args) + [pl.BlockSpec(memory_space=pltpu.HBM)] * len(far),
        out_specs=[near] * len(outs),
        scratch_shapes=list(scratch),
        compiler_params=pltpu.CompilerParams(vmem_limit_bytes=16 * 1024 * 1024),
    )(
        *[pltpu.with_memory_space_constraint(a, pltpu.VMEM) for a in args],
        *[pltpu.with_memory_space_constraint(a, pltpu.HBM) for a in far],
    )


def fetched(sources, targets, semaphores):
    copies = [
        pltpu.make_async_copy(source, target, semaphores.at[i])
        for i, (source, target) in enumerate(zip(sources, targets, strict=True))
    ]
    for copy in copies:
        copy.start()
    return copies


def dot(a, b):
    return jnp.dot(a, b, preferred_element_type=f32)


def dot_t(a, b):
    return lax.dot_general(a, b, (((1,), (1,)), ((), ())), preferred_element_type=f32)


def lane(shape):
    return lax.broadcasted_iota(jnp.int32, shape, len(shape) - 1)


def down_kernel(*refs):
    far, (out, send), near, sems = refs[:6], refs[6:8], refs[8:14], refs[14]
    copies = fetched(far, near, sems)
    tokens, gain, w_q, w_kv, w_rope, w_out = near
    copies[0].wait()
    copies[1].wait()
    resid = tokens[...].astype(f32)
    scaled = (resid * gain[...].astype(f32)[None, :]).astype(bf16)
    q, kv = w_q.shape[1], w_kv.shape[1]
    copies[2].wait()
    out[:, :q] = dot(scaled, w_q[...])
    copies[3].wait()
    out[:, q : q + kv] = dot(scaled, w_kv[...])
    copies[4].wait()
    tail = dot_t(scaled, w_rope[...])
    square = jnp.sum(resid * resid, axis=1, keepdims=True)
    rest = LANES - tail.shape[1]
    out[:, q + kv :] = jnp.concatenate(
        [tail, jnp.broadcast_to(square, (tail.shape[0], rest))], axis=1
    )
    copies[5].wait()
    send[...] = w_out[...].astype(f32)


def fetch_kernel(*refs):
    count = (len(refs) - 2) // 2
    for copy in fetched(refs[1 : 1 + count], refs[1 + count : -1], refs[-1]):
        copy.wait()


def normed(values, gain):
    return values * lax.rsqrt(jnp.mean(values * values, axis=-1, keepdims=True) + EPS) * gain


def gathered(ref, start, count, stride):
    return jnp.concatenate(
        [ref[c, pl.ds(start, count, stride=stride), :] for c in range(ref.shape[0])], axis=1
    )


def rotate(values, cosine, sine, size):
    low = lane(values.shape) % size < size // 2
    other = jnp.where(
        low, pltpu.roll(values, LANES - size // 2, 1), pltpu.roll(values, size // 2, 1)
    )
    return values * cosine + other * sine


def attend_kernel(
    heads,
    sums,
    gain_q,
    gain_kv,
    cosine,
    sine,
    angle,
    w_nope,
    w_rope,
    w_key,
    w_value,
    latent,
    rope,
    new_latent,
    new_rope,
    queries,
    keep,
    give,
    accs,
    scored,
):
    n_seq, rows, kr = latent.shape
    rp = rope.shape[1]
    qr = gain_q.shape[0]
    nope = w_key.shape[0] // heads
    vs = w_value.shape[0] // heads
    scale = (nope + rp) ** (-0.5)
    tail = sums[:, qr + kr :]
    inv_in = lax.rsqrt(tail[:, LANES - 1 :] / D + EPS)
    query_latent = normed(inv_in * sums[:, :qr], gain_q[...].astype(f32)[None, :]).astype(bf16)
    new_latent[...] = normed(inv_in * sums[:, qr : qr + kr], gain_kv[...].astype(f32)[None, :]).astype(bf16)
    rotated = rotate(inv_in * tail, cosine[...], sine[...], rp)
    new_rope[...] = rotated[:, :rp].astype(bf16)
    up = dot_t(query_latent, w_nope[...])
    per = MXU // nope
    for g in range(heads // per):
        part = up[:, g * MXU : (g + 1) * MXU]
        block = lane(part.shape) // nope
        lhs = jnp.concatenate([jnp.where(block == i, part, 0.0) for i in range(per)], axis=0)
        wide = dot(lhs.astype(bf16), w_key[g * MXU : (g + 1) * MXU, :])
        for c in range(kr // LANES):
            queries[c, g * per * n_seq : (g + 1) * per * n_seq, :] = wide[
                :, c * LANES : (c + 1) * LANES
            ]
    turned = dot_t(query_latent, w_rope[...])
    rotated = jnp.concatenate(
        [
            rotate(turned[:, i : i + LANES], cosine[...], sine[...], rp)
            for i in range(0, heads * rp, LANES)
        ],
        axis=1,
    )
    for h in range(heads):
        queries[kr // LANES, h * n_seq : (h + 1) * n_seq, :rp] = rotated[:, h * rp : (h + 1) * rp]
    first = (lax.axis_index("kv") * lax.axis_size("tp") + lax.axis_index("tp")) * rows
    position = (first + lane((heads, rows))).astype(f32)
    low = lane((heads, LANES)) < LANES // 2
    for s in range(n_seq):
        own = gathered(queries, s, heads, n_seq).astype(bf16)
        scored[s] = (
            dot_t(own[:, :kr], latent[s]) + dot(own[:, kr : kr + rp], rope[s])
        ) * scale
    for s in range(n_seq):
        live = position < angle[s : s + 1, 0:1]
        scores = jnp.where(live, scored[s], -1e30)
        top = jnp.max(scores, axis=1, keepdims=True)
        weights = jnp.where(live, jnp.exp(scores - top), 0.0)
        total = jnp.sum(weights, axis=1, keepdims=True)
        scored[s] = weights
        accs[kr // LANES, s * heads : (s + 1) * heads, :] = jnp.where(low, top, total)
    for s in range(n_seq):
        acc = dot(scored[s].astype(bf16), latent[s])
        for c in range(kr // LANES):
            accs[c, s * heads : (s + 1) * heads, :] = acc[:, c * LANES : (c + 1) * LANES]
    per = MXU // vs
    groups = []
    for g in range(heads // per):
        acc = jnp.concatenate(
            [gathered(accs, g * per + i, n_seq, heads)[:, :kr] for i in range(per)], axis=0
        )
        coarse = acc.astype(bf16)
        fine = (acc - coarse.astype(f32)).astype(bf16)
        wide = dot_t(
            jnp.concatenate([coarse, fine], axis=0), w_value[g * MXU : (g + 1) * MXU, :]
        )
        wide = wide[: per * n_seq] + wide[per * n_seq :]
        block = lane((n_seq, MXU)) // vs
        groups.append(
            sum(
                jnp.where(block == i, wide[i * n_seq : (i + 1) * n_seq, :], 0.0)
                for i in range(per)
            )
        )
    in_half = heads // 2
    place = lane((n_seq, LANES)) % (LANES // 2)
    halves = []
    for half in range(2):
        stats = jnp.zeros((n_seq, LANES), f32)
        for i in range(in_half):
            each = accs[kr // LANES, pl.ds(half * in_half + i, n_seq, stride=heads), :]
            stats = jnp.where(place == i, each, stats)
        mine = groups[half * len(groups) // 2 : (half + 1) * len(groups) // 2]
        halves.append(jnp.concatenate(mine + [stats], axis=1))
    upper = parity() == 1
    keep[...] = jnp.where(upper, halves[1], halves[0])
    give[...] = jnp.where(upper, halves[0], halves[1])


def spread(factor, heads, width):
    n_seq = factor.shape[0]
    per = LANES // width
    block = lane((n_seq, LANES)) // width
    tiles = []
    for g in range(heads // per):
        tile = jnp.broadcast_to(factor[:, g * per : g * per + 1], (n_seq, LANES))
        for i in range(1, per):
            tile = jnp.where(block == i, factor[:, g * per + i : g * per + i + 1], tile)
        tiles.append(tile)
    return jnp.concatenate(tiles, axis=1)


def merge_kernel(in_half, one, two, out):
    body = one.shape[1] - LANES
    low = lane((one.shape[0], LANES)) < LANES // 2
    stats_one, stats_two = one[:, body:], two[:, body:]
    top = jnp.where(low, jnp.maximum(stats_one, stats_two), 0.0)
    fade_one = jnp.exp(jnp.where(low, stats_one - top, 0.0))
    fade_two = jnp.exp(jnp.where(low, stats_two - top, 0.0))
    total = stats_one * pltpu.roll(fade_one, LANES // 2, 1) + stats_two * pltpu.roll(
        fade_two, LANES // 2, 1
    )
    out[:, body:] = jnp.where(low, top, total)
    width = body // in_half
    out[:, :body] = one[:, :body] * spread(fade_one, in_half, width) + two[:, :body] * spread(
        fade_two, in_half, width
    )


def self_kernel(heads, nope, new_latent, new_rope, queries, w_value, scores, values):
    n_seq, kr = new_latent.shape
    rp = new_rope.shape[1]
    scale = (nope + rp) ** (-0.5)
    key, key_rope = new_latent[...].astype(f32), new_rope[...].astype(f32)
    in_half = heads // 2
    where = lane((n_seq, LANES))
    for half in range(2):
        tile = jnp.zeros((n_seq, LANES), f32)
        for i in range(in_half):
            h = half * in_half + i
            query = jnp.concatenate(
                [queries[c, h * n_seq : (h + 1) * n_seq, :] for c in range(queries.shape[0])],
                axis=1,
            )
            query = query.astype(bf16).astype(f32)
            score = jnp.sum(query[:, :kr] * key, axis=1, keepdims=True) + jnp.sum(
                query[:, kr : kr + rp] * key_rope, axis=1, keepdims=True
            )
            tile = jnp.where(where == i, score * scale, tile)
        scores[half] = tile
    values[...] = dot_t(new_latent[...], w_value[...])


def middle_kernel(
    heads, *refs
):
    (own, other, self_scores, self_values, tokens, gain, w_in), refs = refs[:7], refs[7:]
    n_tp = lax.axis_size("tp")
    w_outs, (mid, keep, give, outs) = refs[:n_tp], refs[n_tp:]
    n_seq = tokens.shape[0]
    in_half = heads // 2
    body = own.shape[1] - LANES
    width = body // in_half
    low = lane((n_seq, LANES)) < LANES // 2
    upper = parity() == 1
    group = w_outs[0].shape[0]
    for half in range(2):
        mine = upper if half == 1 else jnp.logical_not(upper)
        part = jnp.where(mine, own[...], other[...])
        stats = part[:, body:]
        scores = self_scores[half]
        top = jnp.where(low, jnp.maximum(stats, scores), 0.0)
        fade = jnp.exp(jnp.where(low, stats - top, 0.0))
        weight = jnp.exp(jnp.where(low, scores - top, 0.0))
        total = pltpu.roll(stats, LANES // 2, 1) * fade + weight
        total = jnp.where(low, total, 1.0)
        values = self_values[:, half * body : (half + 1) * body]
        joined = part[:, :body] * spread(fade / total, in_half, width) + values * spread(
            weight.astype(bf16).astype(f32) / total, in_half, width
        )
        joined = joined.astype(bf16)
        for g in range(body // group):
            outs[half * (body // group) + g] = joined[:, g * group : (g + 1) * group]
    me = lax.axis_index("tp")
    attn = dot(outs[me], w_outs[0][...].astype(bf16))
    for m in range(1, n_tp):
        attn += dot(outs[jnp.bitwise_xor(me, m)], w_outs[m][...].astype(bf16))
    resid_mid = tokens[...].astype(f32) + attn
    mid[...] = resid_mid
    scaled = (resid_mid * gain[...].astype(f32)[None, :]).astype(bf16)
    square = jnp.broadcast_to(jnp.sum(resid_mid * resid_mid, axis=1, keepdims=True), (n_seq, LANES))
    hidden = dot(scaled, w_in[...])
    half = hidden.shape[1] // 2
    keep[:, :half] = jnp.where(upper, hidden[:, half:], hidden[:, :half])
    give[:, :half] = jnp.where(upper, hidden[:, :half], hidden[:, half:])
    keep[:, half:] = square
    give[:, half:] = square


def last_kernel(own, other, w_out, out):
    half = own.shape[1] - LANES
    inv_mid = lax.rsqrt(own[:, half : half + 1] / D + EPS)
    mine = parity()
    total = None
    for part, place in ((own, mine), (other, 1 - mine)):
        hidden = jnp.square(jax.nn.relu(inv_mid * part[:, :half])).astype(bf16)
        begin = pl.multiple_of(place * half, half)
        term = dot(hidden, w_out[pl.ds(begin, half), :])
        total = term if total is None else total + term
    out[...] = total


def per_device(
    tokens,
    lengths,
    latent_cache,
    rope_cache,
    gain_in,
    w_down_q,
    w_down_kv,
    w_rope_key,
    gain_q,
    w_up_qn,
    w_up_qr,
    gain_kv,
    w_key_up,
    w_value_up,
    w_attn_out,
    gain_mid,
    w_ff_in,
    w_ff_out,
):
    n_seq = tokens.shape[0]
    qr, heads, nope = w_up_qn.shape
    rp = w_up_qr.shape[2]
    kr, _, vs = w_value_up.shape
    d_dev = tokens.shape[1]
    w_nope = w_up_qn.transpose(1, 2, 0).reshape(heads * nope, qr)
    w_rope = w_up_qr.transpose(1, 2, 0).reshape(heads * rp, qr)
    w_key = w_key_up.transpose(1, 2, 0).reshape(heads * nope, kr)
    w_value = w_value_up.transpose(1, 2, 0).reshape(heads * vs, kr)
    index = np.arange(LANES) % rp
    inverse = (10000.0 ** (-(index % (rp // 2)) / (rp // 2))).astype(np.float32)
    sign = np.where(index < rp // 2, -1.0, 1.0).astype(np.float32)
    angle = lengths.astype(f32)[:, None] * inverse[None, :]
    cosine, sine = jnp.cos(angle), jnp.sin(angle) * sign
    w_out_own = w_attn_out.reshape(-1, d_dev)

    first_far = (tokens, gain_in, w_down_q, w_down_kv, w_rope_key.T, w_out_own)
    sums, w_send = call(
        down_kernel,
        [((n_seq, qr + kr + LANES), f32), (w_out_own.shape, f32)],
        scratch=[pltpu.VMEM(a.shape, a.dtype) for a in first_far]
        + [pltpu.SemaphoreType.DMA((len(first_far),))],
        far=first_far,
    )
    crossed = [bit | 1 for bit in higher_bits("kv", 1)]
    w_outs = [w_out_own]
    unsent = list(range(1, lax.axis_size("tp")))

    def send(after, count):
        held, after = lax.optimization_barrier((w_send, after))
        for m in unsent[:count]:
            w_outs.append(swap(held, 0, m))
        del unsent[:count]
        return after

    for mask in [1] + crossed:
        sums = sums + swap(sums, mask)
        if mask == 1:
            sums = send(sums, 1)
        if mask == crossed[0]:
            early = sums
    far = (
        gain_q,
        gain_kv,
        w_nope,
        w_rope,
        w_key,
        w_value,
        latent_cache,
        rope_cache.transpose(0, 2, 1),
        tokens,
        gain_mid,
    )
    gain_q, gain_kv, w_nope, w_rope, w_key, w_value, latent_cache, rope_cache, *kept = call(
        fetch_kernel,
        [(a.shape, a.dtype) for a in far],
        early,
        scratch=[pltpu.SemaphoreType.DMA((len(far),))],
        far=far,
    )
    in_half = heads // 2
    state = (n_seq, in_half * vs + LANES)
    new_latent, new_rope, queries, keep, give = call(
        functools.partial(attend_kernel, heads),
        [
            ((n_seq, kr), bf16),
            ((n_seq, rp), bf16),
            ((kr // LANES + 1, heads * n_seq, LANES), f32),
            (state, f32),
            (state, f32),
        ],
        sums,
        gain_q,
        gain_kv,
        cosine,
        sine,
        angle,
        w_nope,
        w_rope,
        w_key,
        w_value,
        latent_cache,
        rope_cache,
        scratch=[
            pltpu.VMEM((kr // LANES + 1, n_seq * heads, LANES), f32),
            pltpu.VMEM((n_seq, heads, latent_cache.shape[1]), f32),
        ],
    )
    self_scores, self_values = call(
        functools.partial(self_kernel, heads, nope),
        [((2, n_seq, LANES), f32), ((n_seq, heads * vs), f32)],
        new_latent,
        new_rope,
        queries,
        w_value,
    )

    def merge(one, two):
        return call(functools.partial(merge_kernel, in_half), [(state, f32)], one, two)[0]

    part = merge(keep, swap(give, 1))
    for mask in crossed:
        part = send(part, 1 if mask == crossed[0] else len(unsent))
        part = merge(part, swap(part, mask))
    for bit in higher_bits("tp", 0):
        part = merge(part, swap(part, 1, bit))
    other = swap(part, 1)
    half = (n_seq, w_ff_in.shape[1] // 2 + LANES)
    resid_mid, keep, give = call(
        functools.partial(middle_kernel, heads),
        [((n_seq, d_dev), f32), (half, f32), (half, f32)],
        part,
        other,
        self_scores,
        self_values,
        *kept,
        w_ff_in,
        *w_outs,
        scratch=[pltpu.VMEM((lax.axis_size("tp"), n_seq, w_out_own.shape[0]), bf16)],
    )
    sums = keep + swap(give, 1)
    for mask in crossed:
        sums = sums + swap(sums, mask)
    (out,) = call(last_kernel, [((n_seq, d_dev), f32)], sums, swap(sums, 1), w_ff_out)
    for bit in higher_bits("tp", 0):
        out = out + swap(out, 0, bit)
    mixed = (resid_mid + out).astype(bf16)
    return (mixed, new_latent, new_rope)


def solution(mesh):
    return jax.shard_map(
        per_device,
        mesh=mesh,
        in_specs=(
            P(None, "kv"),
            P(),
            P(None, ("kv", "tp"), None),
            P(None, ("kv", "tp"), None),
            P("kv"),
            P("kv", None),
            P("kv", None),
            P("kv", None),
            P(),
            P(),
            P(),
            P(),
            P(),
            P(),
            P("tp", None, "kv"),
            P("kv"),
            P("kv", "tp"),
            P("tp", "kv"),
        ),
        out_specs=(P(None, "kv"), P(), P()),
        check_vma=False,
    )
```

time: 219 us -> 62.7 us (0.29)
  blocking collectives: 117 us -> 0 us
  waiting for transfers between devices: 51.5 us -> 25.8 us
  starting transfers between devices: 12.1 us -> 26.5 us
  between operations: 14.2 us -> 0.77 us
  matrix products: 8.74 us -> 0 us
  Pallas kernels: 0 us -> 7.33 us
  other arithmetic: 7.81 us -> 0.79 us
  local copies, waits for them, and re-layouts: 6.26 us -> 1.23 us
    psum x4 -> x0, blocking collectives: 76.9 us -> none  [the longest x1 30.8 us: per_device(): lax.psum((part_q, part_kv, part_rope, square_in), 'kv')]
    psum x1 -> x0, waiting for transfers between devices: 51.4 us -> none  [per_device(): hidden_sum, total_mid = lax.psum((hidden_part, square_mid), 'kv')]
    all_gather x3 -> x0, blocking collectives: 40.6 us -> none  [combined_all(): gathered = jax.tree.map(lambda a: lax.all_gather(a, axis), part)]
    ppermute x0 -> x18, starting transfers between devices: none -> 26.5 us  [swap(): return lax.ppermute(value, BOTH, pairs)]
    ppermute x0 -> x18, waiting for transfers between devices: none -> 25.8 us  [swap(): return lax.ppermute(value, BOTH, pairs)]
    all_to_all x3 -> x0, starting transfers between devices: 12.1 us -> none  [the longest x1 4.19 us: per_device(): lax.all_to_all(total[None], 'tp', split_axis=2, concat_axis=0, tiled=True)]
    dot_general x14 -> x0, matrix products: 8.74 us -> none  [the longest x1 1.19 us: per_device(): out_part = jnp.dot(hidden, w_ff_out, preferred_element_type=f32)]
    pallas_call x0 -> x11, Pallas kernels: none -> 7.33 us  [call(): pl.pallas_call(kernel, out_shape=[pltpu.VMEM(s, t) for s, t in outs], in_...]
  transfers between devices with their start and end apart: 4 -> 18, of which waited for: 1 -> 13; matrix products, arithmetic and copies ran while one was open for 2% -> 2% of each run, Pallas kernels for 0% -> 5%
where the time goes in v2:
time: 62.7 us; the launch traced here: 62.5 us
  starting transfers between devices  26.5 us (42%)
  waiting for transfers between devices  25.8 us (41%)
  Pallas kernels  7.33 us (12%)
  local copies, waits for them, and re-layouts  1.23 us (2%)
  other arithmetic  0.79 us (1%)
  between operations  0.77 us (1%)
    ppermute x18, starting transfers between devices, swap(): return lax.ppermute(value, BOTH, pairs)  26.5 us
    ppermute x18, waiting for transfers between devices, swap(): return lax.ppermute(value, BOTH, pairs)  25.8 us
    pallas_call x11, Pallas kernels, call(): pl.pallas_call(kernel, out_shape=[pltpu.VMEM(s, t) for s, t in outs], in_...  7.33 us
  transfers between devices with their start and end apart: 18, of which 13 were waited for; matrix products, arithmetic and copies ran while one was open for 2% of the time, Pallas kernels for 5%

profile of v2, /device:TPU:0, one launch (start us, length us, event | category | flops | bytes accessed | tf_op | source)
XLA Modules:
  0.0 62.5 jit_solution(1950034738961527500)
XLA Ops:
  0.6 1.5 %shard_map.211 = (f32[16,896]{1,0:T(8,128)S(1)}, f32[256,256]{1,0:T(8,128)S(1)}) custom-call(bf16[16,256]{1,0:T(8,128)(2,1)} %refs_9_.1, bf16[256]{0:T(256)(128)(2,1)} %refs_1_.2, bf16[256,512]{1,0:T(8,128)(2,1)} %refs_2_.2, bf16[256,256]{1,0:T(8,128)(2,1)} %refs_3_.1, bf16[32,256]{1,0:T(8,128)(2,1)} %bitcast.22, bf16[256,256]{1,0:T(8,128)(2,1)} %bitcast.15), custom_call_target="tpu_custom_call" | custom-call | tf_op jit(solution)/shard_map/pallas_call | solution.py:45
  2.1 0.6 collective-permute-start
  2.7 0.9 %collective-permute-done = f32[16,896]{1,0:T(8,128)S(1)} collective-permute-done((f32[16,896]{1,0:T(8,128)S(1)}, f32[16,896]{1,0:T(8,128)S(1)}, u32[]{:S(2)}, u32[]{:S(2)}) %collective-permute-start) | collective-permute-done | bytes 57376 | tf_op jit(solution)/shard_map/ppermute | solution.py:25
  3.6 2.7 %collective-permute-start.1 = (f32[16,896]{1,0:T(8,128)S(1)}, f32[16,896]{1,0:T(8,128)S(1)}, u32[]{:S(2)}, u32[]{:S(2)}) collective-permute-start(f32[16,896]{1,0:T(8,128)S(1)} %add.27), channel_id=1, source_target_pairs={{0,12},{1,13},{2,14},{3,15},{4,8},{5,9},{6,10},{7,11},{8,4},{9,5},... | collective-permute-start | bytes 172040 | tf_op jit(solution)/shard_map/ppermute | solution.py:25
  6.3 2.0 %collective-permute-done.1 = f32[16,896]{1,0:T(8,128)S(1)} collective-permute-done((f32[16,896]{1,0:T(8,128)S(1)}, f32[16,896]{1,0:T(8,128)S(1)}, u32[]{:S(2)}, u32[]{:S(2)}) %collective-permute-start.1) | collective-permute-done | bytes 57376 | tf_op jit(solution)/shard_map/ppermute | solution.py:25
  8.3 3.0 %collective-permute-start.2 = (f32[16,896]{1,0:T(8,128)S(1)}, f32[16,896]{1,0:T(8,128)S(1)}, u32[]{:S(2)}, u32[]{:S(2)}) collective-permute-start(f32[16,896]{1,0:T(8,128)S(1)} %add.28.refs_0_), channel_id=1, source_target_pairs={{0,20},{1,21},{2,22},{3,23},{4,16},{5,17},{6,18},{7,19},{8,28},{9,... | collective-permute-start | bytes 172040 | tf_op jit(solution)/shard_map/ppermute | solution.py:25
  11.3 0.1 broadcast_multiply_fusion
  11.4 2.1 %shard_map.212 = (bf16[512]{0:T(512)(128)(2,1)S(1)}, bf16[256]{0:T(256)(128)(2,1)S(1)}, bf16[1024,512]{1,0:T(8,128)(2,1)S(1)}, bf16[512,512]{1,0:T(8,128)(2,1)S(...) custom-call(f32[16,896]{1,0:T(8,128)S(1)} %add.28.refs_0_, ...), custom_call_target="tpu_custom_call" | custom-call | tf_op jit(solution)/shard_map/pallas_call | solution.py:45
  13.5 1.9 %shard_map.213 = (bf16[16,256]{1,0:T(8,128)(2,1)S(1)}, bf16[16,32]{1,0:T(8,128)(2,1)S(1)}, f32[3,256,128]{2,1,0:T(8,128)S(1)}, f32[16,640]{1,0:T(8,128)S(1)}, f32[16,640]{1,0:T(8,128)S(1)}) custom-call(f32[16,896]{1,0:T(8,128)S(1)} %add.29.sums, bf16[512]{0:T(512)(128)(2,1)S(1)} %get-tuple-element.34.gain_q, bf16[256]{0:T(256)(128)(2,1)S(1)} %get-tuple-element.35.gain_kv, ...), custom_call_target="tpu_custom_call" | custom-call | tf_op jit(solution)/shard_map/pallas_call | solution.py:45
  15.4 0.0 copy-start
  15.4 0.4 collective-permute-start.3
  15.8 0.9 %collective-permute-done.3.two = f32[16,640]{1,0:T(8,128)S(1)} collective-permute-done((f32[16,640]{1,0:T(8,128)S(1)}, f32[16,640]{1,0:T(8,128)S(1)}, u32[]{:S(2)}, u32[]{:S(2)}) %collective-permute-start.3) | collective-permute-done | bytes 40992 | tf_op jit(solution)/shard_map/ppermute | solution.py:25
  16.7 0.1 shard_map.214.one
  16.8 2.3 %collective-permute-start.4 = (f32[16,640]{1,0:T(8,128)S(1)}, f32[16,640]{1,0:T(8,128)S(1)}, u32[]{:S(2)}, u32[]{:S(2)}) collective-permute-start(f32[16,640]{1,0:T(8,128)S(1)} %shard_map.214.one), channel_id=1, source_target_pairs={{0,12},{1,13},{2,14},{3,15},{4,8},{5,9},{6,10},{7,11},{8,4},{9,5},... | collective-permute-start | bytes 122888 | tf_op jit(solution)/shard_map/ppermute | solution.py:25
  19.1 1.5 %collective-permute-start.9 = (f32[256,256]{1,0:T(8,128)S(1)}, f32[256,256]{1,0:T(8,128)S(1)}, u32[]{:S(2)}, u32[]{:S(2)}) collective-permute-start(f32[256,256]{1,0:T(8,128)S(1)} %get-tuple-element.55), channel_id=1, source_target_pairs={{0,1},{1,0},{2,3},{3,2},{4,5},{5,4},{6,7},{7,6},{8,9},{9,8},{10,11... | collective-permute-start | bytes 786440 | tf_op jit(solution)/shard_map/ppermute | solution.py:25
  20.6 1.5 %collective-permute-start.10 = (f32[256,256]{1,0:T(8,128)S(1)}, f32[256,256]{1,0:T(8,128)S(1)}, u32[]{:S(2)}, u32[]{:S(2)}) collective-permute-start(f32[256,256]{1,0:T(8,128)S(1)} %get-tuple-element.55), channel_id=1, source_target_pairs={{0,2},{1,3},{2,0},{3,1},{4,6},{5,7},{6,4},{7,5},{8,10},{9,11},{10,... | collective-permute-start | bytes 786440 | tf_op jit(solution)/shard_map/ppermute | solution.py:25
  22.1 0.1 shard_map.215.one
  22.3 1.9 %collective-permute-start.11 = (f32[256,256]{1,0:T(8,128)S(1)}, f32[256,256]{1,0:T(8,128)S(1)}, u32[]{:S(2)}, u32[]{:S(2)}) collective-permute-start(f32[256,256]{1,0:T(8,128)S(1)} %get-tuple-element.55), channel_id=1, source_target_pairs={{0,3},{1,2},{2,1},{3,0},{4,7},{5,6},{6,5},{7,4},{8,11},{9,10},{10,... | collective-permute-start | bytes 786440 | tf_op jit(solution)/shard_map/ppermute | solution.py:25
  24.2 2.2 %collective-permute-start.5 = (f32[16,640]{1,0:T(8,128)S(1)}, f32[16,640]{1,0:T(8,128)S(1)}, u32[]{:S(2)}, u32[]{:S(2)}) collective-permute-start(f32[16,640]{1,0:T(8,128)S(1)} %shard_map.215.one), channel_id=1, source_target_pairs={{0,20},{1,21},{2,22},{3,23},{4,16},{5,17},{6,18},{7,19},{8,28},{9,... | collective-permute-start | bytes 122888 | tf_op jit(solution)/shard_map/ppermute | solution.py:25
  26.5 2.3 %collective-permute-done.5.two = f32[16,640]{1,0:T(8,128)S(1)} collective-permute-done((f32[16,640]{1,0:T(8,128)S(1)}, f32[16,640]{1,0:T(8,128)S(1)}, u32[]{:S(2)}, u32[]{:S(2)}) %collective-permute-start.5) | collective-permute-done | bytes 40992 | tf_op jit(solution)/shard_map/ppermute | solution.py:25
  28.7 0.1 shard_map.216.one
  28.9 0.4 collective-permute-start.6
  29.3 4.4 %collective-permute-done.6.two = f32[16,640]{1,0:T(8,128)S(1)} collective-permute-done((f32[16,640]{1,0:T(8,128)S(1)}, f32[16,640]{1,0:T(8,128)S(1)}, u32[]{:S(2)}, u32[]{:S(2)}) %collective-permute-start.6) | collective-permute-done | bytes 40992 | tf_op jit(solution)/shard_map/ppermute | solution.py:25
  33.6 0.1 shard_map.217.one
  33.7 1.9 %collective-permute-start.7 = (f32[16,640]{1,0:T(8,128)S(1)}, f32[16,640]{1,0:T(8,128)S(1)}, u32[]{:S(2)}, u32[]{:S(2)}) collective-permute-start(f32[16,640]{1,0:T(8,128)S(1)} %shard_map.217.one), channel_id=1, source_target_pairs={{0,6},{1,7},{2,4},{3,5},{4,2},{5,3},{6,0},{7,1},{8,14},{9,15},{10,... | collective-permute-start | bytes 122888 | tf_op jit(solution)/shard_map/ppermute | solution.py:25
  35.7 1.7 %collective-permute-done.7.two = f32[16,640]{1,0:T(8,128)S(1)} collective-permute-done((f32[16,640]{1,0:T(8,128)S(1)}, f32[16,640]{1,0:T(8,128)S(1)}, u32[]{:S(2)}, u32[]{:S(2)}) %collective-permute-start.7) | collective-permute-done | bytes 40992 | tf_op jit(solution)/shard_map/ppermute | solution.py:25
  37.4 0.1 shard_map.218.refs_0_
  37.5 0.7 %collective-permute-start.8 = (f32[16,640]{1,0:T(8,128)S(1)}, f32[16,640]{1,0:T(8,128)S(1)}, u32[]{:S(2)}, u32[]{:S(2)}) collective-permute-start(f32[16,640]{1,0:T(8,128)S(1)} %shard_map.218.refs_0_), channel_id=1, source_target_pairs={{0,4},{1,5},{2,6},{3,7},{4,0},{5,1},{6,2},{7,3},{8,12},{9,13},{10,... | collective-permute-start | bytes 122888 | tf_op jit(solution)/shard_map/ppermute | solution.py:25
  38.2 0.3 shard_map.219
  38.4 0.6 collective-permute-done.8.refs_1_
  39.1 0.0 copy-done.2
  39.1 0.7 %shard_map.220 = (f32[16,256]{1,0:T(8,128)S(1)}, f32[16,1152]{1,0:T(8,128)S(1)}, f32[16,1152]{1,0:T(8,128)S(1)}) custom-call(f32[16,640]{1,0:T(8,128)S(1)} %shard_map.218.refs_0_, f32[16,640]{1,0:T(8,128)S(1)} %collective-permute-done.8.refs_1_, f32[2,16,128]{2,1,0:T(8,128)S(1)} %get-tuple-element.49.refs_2_, f32[16,1024]{1,0:T(8,128)S(1)} %get-tuple-element.50.refs_3_, ...), custom_call_target="tpu_custom_call" | custom-call | tf_op jit(solution)/shard_map/pallas_call | solution.py:45
  39.8 0.4 collective-permute-start.12
  40.2 0.9 %collective-permute-done.12 = f32[16,1152]{1,0:T(8,128)S(1)} collective-permute-done((f32[16,1152]{1,0:T(8,128)S(1)}, f32[16,1152]{1,0:T(8,128)S(1)}, u32[]{:S(2)}, u32[]{:S(2)}) %collective-permute-start.12) | collective-permute-done | bytes 73760 | tf_op jit(solution)/shard_map/ppermute | solution.py:25
  41.1 0.6 collective-permute-start.13
  41.7 3.5 %collective-permute-done.13 = f32[16,1152]{1,0:T(8,128)S(1)} collective-permute-done((f32[16,1152]{1,0:T(8,128)S(1)}, f32[16,1152]{1,0:T(8,128)S(1)}, u32[]{:S(2)}, u32[]{:S(2)}) %collective-permute-start.13) | collective-permute-done | bytes 73760 | tf_op jit(solution)/shard_map/ppermute | solution.py:25
  45.3 3.4 %collective-permute-start.14 = (f32[16,1152]{1,0:T(8,128)S(1)}, f32[16,1152]{1,0:T(8,128)S(1)}, u32[]{:S(2)}, u32[]{:S(2)}) collective-permute-start(f32[16,1152]{1,0:T(8,128)S(1)} %add.31), channel_id=1, source_target_pairs={{0,20},{1,21},{2,22},{3,23},{4,16},{5,17},{6,18},{7,19},{8,28},{9,... | collective-permute-start | bytes 221192 | tf_op jit(solution)/shard_map/ppermute | solution.py:25
  48.6 4.1 %collective-permute-done.14 = f32[16,1152]{1,0:T(8,128)S(1)} collective-permute-done((f32[16,1152]{1,0:T(8,128)S(1)}, f32[16,1152]{1,0:T(8,128)S(1)}, u32[]{:S(2)}, u32[]{:S(2)}) %collective-permute-start.14) | collective-permute-done | bytes 73760 | tf_op jit(solution)/shard_map/ppermute | solution.py:25
  52.8 0.2 collective-permute-start.15
  52.9 1.2 %collective-permute-done.15.other = f32[16,1152]{1,0:T(8,128)S(1)} collective-permute-done((f32[16,1152]{1,0:T(8,128)S(1)}, f32[16,1152]{1,0:T(8,128)S(1)}, u32[]{:S(2)}, u32[]{:S(2)}) %collective-permute-start.15) | collective-permute-done | bytes 73760 | tf_op jit(solution)/shard_map/ppermute | solution.py:25
  54.1 0.3 shard_map.221
  54.4 1.4 %collective-permute-start.16 = (f32[16,256]{1,0:T(8,128)S(1)}, f32[16,256]{1,0:T(8,128)S(1)}, u32[]{:S(2)}, u32[]{:S(2)}) collective-permute-start(f32[16,256]{1,0:T(8,128)S(1)} %shard_map.221), channel_id=1, source_target_pairs={{0,1},{1,0},{2,3},{3,2},{4,5},{5,4},{6,7},{7,6},{8,9},{9,8},{10,11... | collective-permute-start | bytes 49160 | tf_op jit(solution)/shard_map/ppermute | solution.py:25
  55.8 2.3 %collective-permute-done.16 = f32[16,256]{1,0:T(8,128)S(1)} collective-permute-done((f32[16,256]{1,0:T(8,128)S(1)}, f32[16,256]{1,0:T(8,128)S(1)}, u32[]{:S(2)}, u32[]{:S(2)}) %collective-permute-start.16) | collective-permute-done | bytes 16416 | tf_op jit(solution)/shard_map/ppermute | solution.py:25
  58.1 1.4 %collective-permute-start.17 = (f32[16,256]{1,0:T(8,128)S(1)}, f32[16,256]{1,0:T(8,128)S(1)}, u32[]{:S(2)}, u32[]{:S(2)}) collective-permute-start(f32[16,256]{1,0:T(8,128)S(1)} %add.33), channel_id=1, source_target_pairs={{0,2},{1,3},{2,0},{3,1},{4,6},{5,7},{6,4},{7,5},{8,10},{9,11},{10,... | collective-permute-start | bytes 49160 | tf_op jit(solution)/shard_map/ppermute | solution.py:25
  59.6 0.6 copy.23
  60.2 0.6 copy.24
  60.8 1.1 %collective-permute-done.17 = f32[16,256]{1,0:T(8,128)S(1)} collective-permute-done((f32[16,256]{1,0:T(8,128)S(1)}, f32[16,256]{1,0:T(8,128)S(1)}, u32[]{:S(2)}, u32[]{:S(2)}) %collective-permute-start.17) | collective-permute-done | bytes 16416 | tf_op jit(solution)/shard_map/ppermute | solution.py:25
  61.9 0.6 add_convert_fusion
  (23 shorter events, 0.1 us)
Async XLA Ops:
  2.1 1.4 %collective-permute-start = (f32[16,896]{1,0:T(8,128)S(1)}, f32[16,896]{1,0:T(8,128)S(1)}, u32[]{:S(2)}, u32[]{:S(2)}) collective-permute-start(f32[16,896]{1,0:T(8,128)S(1)} %get-tuple-element.32), channel_id=1, source_target_pairs={{0,4},{1,5},{2,6},{3,7},{4,0},{5,1},{6,2},{7,3},{8,12},{9,13},{10,... | collective-permute-start | bytes 172040 | tf_op jit(solution)/shard_map/ppermute | solution.py:25
  3.6 2.7 %copy-start.5 = (s32[16]{0:T(128)S(1)}, s32[16]{0:T(128)}, u32[]{:S(2)}) copy-start(s32[16]{0:T(128)} %param.21) | copy-start | bytes 196
  3.6 4.7 %collective-permute-start.1 = (f32[16,896]{1,0:T(8,128)S(1)}, f32[16,896]{1,0:T(8,128)S(1)}, u32[]{:S(2)}, u32[]{:S(2)}) collective-permute-start(f32[16,896]{1,0:T(8,128)S(1)} %add.27), channel_id=1, source_target_pairs={{0,12},{1,13},{2,14},{3,15},{4,8},{5,9},{6,10},{7,11},{8,4},{9,5},... | collective-permute-start | bytes 172040 | tf_op jit(solution)/shard_map/ppermute | solution.py:25
  6.3 5.0 %copy-start.3 = (f32[128]{0:T(128)S(1)}, f32[128]{0:T(128)}, u32[]{:S(2)}) copy-start(f32[128]{0:T(128)} %constant.5.clone) | copy-start | bytes 1540
  6.3 5.0 %copy-start.4 = (f32[128]{0:T(128)S(1)}, f32[128]{0:T(128)}, u32[]{:S(2)}) copy-start(f32[128]{0:T(128)} %constant.6) | copy-start | bytes 1540
  8.3 5.2 %collective-permute-start.2 = (f32[16,896]{1,0:T(8,128)S(1)}, f32[16,896]{1,0:T(8,128)S(1)}, u32[]{:S(2)}, u32[]{:S(2)}) collective-permute-start(f32[16,896]{1,0:T(8,128)S(1)} %add.28.refs_0_), channel_id=1, source_target_pairs={{0,20},{1,21},{2,22},{3,23},{4,16},{5,17},{6,18},{7,19},{8,28},{9,... | collective-permute-start | bytes 172040 | tf_op jit(solution)/shard_map/ppermute | solution.py:25
  15.4 23.7 %copy-start = (bf16[256,2048]{1,0:T(8,128)(2,1)S(1)}, bf16[256,2048]{1,0:T(8,128)(2,1)}, u32[]{:S(2)}) copy-start(bf16[256,2048]{1,0:T(8,128)(2,1)} %refs_6_.1) | copy-start | bytes 3145732
  15.4 1.3 %collective-permute-start.3 = (f32[16,640]{1,0:T(8,128)S(1)}, f32[16,640]{1,0:T(8,128)S(1)}, u32[]{:S(2)}, u32[]{:S(2)}) collective-permute-start(f32[16,640]{1,0:T(8,128)S(1)} %get-tuple-element.43), channel_id=1, source_target_pairs={{0,4},{1,5},{2,6},{3,7},{4,0},{5,1},{6,2},{7,3},{8,12},{9,13},{10,... | collective-permute-start | bytes 122888 | tf_op jit(solution)/shard_map/ppermute | solution.py:25
  16.8 5.3 %collective-permute-start.4 = (f32[16,640]{1,0:T(8,128)S(1)}, f32[16,640]{1,0:T(8,128)S(1)}, u32[]{:S(2)}, u32[]{:S(2)}) collective-permute-start(f32[16,640]{1,0:T(8,128)S(1)} %shard_map.214.one), channel_id=1, source_target_pairs={{0,12},{1,13},{2,14},{3,15},{4,8},{5,9},{6,10},{7,11},{8,4},{9,5},... | collective-permute-start | bytes 122888 | tf_op jit(solution)/shard_map/ppermute | solution.py:25
  19.1 19.3 %collective-permute-start.9 = (f32[256,256]{1,0:T(8,128)S(1)}, f32[256,256]{1,0:T(8,128)S(1)}, u32[]{:S(2)}, u32[]{:S(2)}) collective-permute-start(f32[256,256]{1,0:T(8,128)S(1)} %get-tuple-element.55), channel_id=1, source_target_pairs={{0,1},{1,0},{2,3},{3,2},{4,5},{5,4},{6,7},{7,6},{8,9},{9,8},{10,11... | collective-permute-start | bytes 786440 | tf_op jit(solution)/shard_map/ppermute | solution.py:25
  20.6 18.4 %collective-permute-start.10 = (f32[256,256]{1,0:T(8,128)S(1)}, f32[256,256]{1,0:T(8,128)S(1)}, u32[]{:S(2)}, u32[]{:S(2)}) collective-permute-start(f32[256,256]{1,0:T(8,128)S(1)} %get-tuple-element.55), channel_id=1, source_target_pairs={{0,2},{1,3},{2,0},{3,1},{4,6},{5,7},{6,4},{7,5},{8,10},{9,11},{10,... | collective-permute-start | bytes 786440 | tf_op jit(solution)/shard_map/ppermute | solution.py:25
  22.3 16.8 %collective-permute-start.11 = (f32[256,256]{1,0:T(8,128)S(1)}, f32[256,256]{1,0:T(8,128)S(1)}, u32[]{:S(2)}, u32[]{:S(2)}) collective-permute-start(f32[256,256]{1,0:T(8,128)S(1)} %get-tuple-element.55), channel_id=1, source_target_pairs={{0,3},{1,2},{2,1},{3,0},{4,7},{5,6},{6,5},{7,4},{8,11},{9,10},{10,... | collective-permute-start | bytes 786440 | tf_op jit(solution)/shard_map/ppermute | solution.py:25
  24.2 4.5 %collective-permute-start.5 = (f32[16,640]{1,0:T(8,128)S(1)}, f32[16,640]{1,0:T(8,128)S(1)}, u32[]{:S(2)}, u32[]{:S(2)}) collective-permute-start(f32[16,640]{1,0:T(8,128)S(1)} %shard_map.215.one), channel_id=1, source_target_pairs={{0,20},{1,21},{2,22},{3,23},{4,16},{5,17},{6,18},{7,19},{8,28},{9,... | collective-permute-start | bytes 122888 | tf_op jit(solution)/shard_map/ppermute | solution.py:25
  28.9 4.7 %collective-permute-start.6 = (f32[16,640]{1,0:T(8,128)S(1)}, f32[16,640]{1,0:T(8,128)S(1)}, u32[]{:S(2)}, u32[]{:S(2)}) collective-permute-start(f32[16,640]{1,0:T(8,128)S(1)} %shard_map.216.one), channel_id=1, source_target_pairs={{0,5},{1,4},{2,7},{3,6},{4,1},{5,0},{6,3},{7,2},{8,13},{9,12},{10,... | collective-permute-start | bytes 122888 | tf_op jit(solution)/shard_map/ppermute | solution.py:25
  33.7 3.6 %collective-permute-start.7 = (f32[16,640]{1,0:T(8,128)S(1)}, f32[16,640]{1,0:T(8,128)S(1)}, u32[]{:S(2)}, u32[]{:S(2)}) collective-permute-start(f32[16,640]{1,0:T(8,128)S(1)} %shard_map.217.one), channel_id=1, source_target_pairs={{0,6},{1,7},{2,4},{3,5},{4,2},{5,3},{6,0},{7,1},{8,14},{9,15},{10,... | collective-permute-start | bytes 122888 | tf_op jit(solution)/shard_map/ppermute | solution.py:25
  37.5 1.5 %collective-permute-start.8 = (f32[16,640]{1,0:T(8,128)S(1)}, f32[16,640]{1,0:T(8,128)S(1)}, u32[]{:S(2)}, u32[]{:S(2)}) collective-permute-start(f32[16,640]{1,0:T(8,128)S(1)} %shard_map.218.refs_0_), channel_id=1, source_target_pairs={{0,4},{1,5},{2,6},{3,7},{4,0},{5,1},{6,2},{7,3},{8,12},{9,13},{10,... | collective-permute-start | bytes 122888 | tf_op jit(solution)/shard_map/ppermute | solution.py:25
  38.2 0.9 %copy-start.2 = (bf16[4,64,256]{2,1,0:T(8,128)(2,1)S(1)}, bf16[4,64,256]{2,1,0:T(8,128)(2,1)}, u32[]{:S(2)}) copy-start(bf16[4,64,256]{2,1,0:T(8,128)(2,1)} %param.34) | copy-start | bytes 393220
  39.1 15.0 %copy-start.1 = (bf16[2048,256]{1,0:T(8,128)(2,1)S(1)}, bf16[2048,256]{1,0:T(8,128)(2,1)}, u32[]{:S(2)}) copy-start(bf16[2048,256]{1,0:T(8,128)(2,1)} %w_out.1) | copy-start | bytes 3145732
  39.8 1.3 %collective-permute-start.12 = (f32[16,1152]{1,0:T(8,128)S(1)}, f32[16,1152]{1,0:T(8,128)S(1)}, u32[]{:S(2)}, u32[]{:S(2)}) collective-permute-start(f32[16,1152]{1,0:T(8,128)S(1)} %get-tuple-element.58), channel_id=1, source_target_pairs={{0,4},{1,5},{2,6},{3,7},{4,0},{5,1},{6,2},{7,3},{8,12},{9,13},{10,... | collective-permute-start | bytes 221192 | tf_op jit(solution)/shard_map/ppermute | solution.py:25
  41.1 4.1 %collective-permute-start.13 = (f32[16,1152]{1,0:T(8,128)S(1)}, f32[16,1152]{1,0:T(8,128)S(1)}, u32[]{:S(2)}, u32[]{:S(2)}) collective-permute-start(f32[16,1152]{1,0:T(8,128)S(1)} %add.30), channel_id=1, source_target_pairs={{0,12},{1,13},{2,14},{3,15},{4,8},{5,9},{6,10},{7,11},{8,4},{9,5},... | collective-permute-start | bytes 221192 | tf_op jit(solution)/shard_map/ppermute | solution.py:25
  45.3 7.5 %collective-permute-start.14 = (f32[16,1152]{1,0:T(8,128)S(1)}, f32[16,1152]{1,0:T(8,128)S(1)}, u32[]{:S(2)}, u32[]{:S(2)}) collective-permute-start(f32[16,1152]{1,0:T(8,128)S(1)} %add.31), channel_id=1, source_target_pairs={{0,20},{1,21},{2,22},{3,23},{4,16},{5,17},{6,18},{7,19},{8,28},{9,... | collective-permute-start | bytes 221192 | tf_op jit(solution)/shard_map/ppermute | solution.py:25
  52.8 1.3 %collective-permute-start.15 = (f32[16,1152]{1,0:T(8,128)S(1)}, f32[16,1152]{1,0:T(8,128)S(1)}, u32[]{:S(2)}, u32[]{:S(2)}) collective-permute-start(f32[16,1152]{1,0:T(8,128)S(1)} %add.32.own), channel_id=1, source_target_pairs={{0,4},{1,5},{2,6},{3,7},{4,0},{5,1},{6,2},{7,3},{8,12},{9,13},{10,... | collective-permute-start | bytes 221192 | tf_op jit(solution)/shard_map/ppermute | solution.py:25
  54.4 3.7 %collective-permute-start.16 = (f32[16,256]{1,0:T(8,128)S(1)}, f32[16,256]{1,0:T(8,128)S(1)}, u32[]{:S(2)}, u32[]{:S(2)}) collective-permute-start(f32[16,256]{1,0:T(8,128)S(1)} %shard_map.221), channel_id=1, source_target_pairs={{0,1},{1,0},{2,3},{3,2},{4,5},{5,4},{6,7},{7,6},{8,9},{9,8},{10,11... | collective-permute-start | bytes 49160 | tf_op jit(solution)/shard_map/ppermute | solution.py:25
  58.1 3.7 %collective-permute-start.17 = (f32[16,256]{1,0:T(8,128)S(1)}, f32[16,256]{1,0:T(8,128)S(1)}, u32[]{:S(2)}, u32[]{:S(2)}) collective-permute-start(f32[16,256]{1,0:T(8,128)S(1)} %add.33), channel_id=1, source_target_pairs={{0,2},{1,3},{2,0},{3,1},{4,6},{5,7},{6,4},{7,5},{8,10},{9,11},{10,... | collective-permute-start | bytes 49160 | tf_op jit(solution)/shard_map/ppermute | solution.py:25

commit v3 on v2

--- a/solution.py
+++ b/solution.py
@@ -8,6 +8,7 @@
 from jax.experimental.pallas import tpu as pltpu
 from jax.sharding import PartitionSpec as P
 
+
 D = 2048
 EPS = 1e-06
 LANES = 128
@@ -29,6 +30,18 @@
     size = lax.axis_size(axis)
     assert size & (size - 1) == 0
     return [1 << i for i in range(first, size.bit_length() - 1)]
+
+
+def paired(terms):
+    while len(terms) > 1:
+        terms = [one + two for one, two in zip(terms[::2], terms[1::2], strict=True)]
+    return terms[0]
+
+
+def tp_rounds():
+    found = higher_bits("tp", 0)
+    pairs = [found[i : i + 2] for i in range(0, len(found), 2)]
+    return [pair + [sum(pair)] if len(pair) == 2 else pair for pair in pairs]
 
 
 def parity():
@@ -78,7 +91,7 @@
 
 
 def down_kernel(*refs):
-    far, (out, send), near, sems = refs[:6], refs[6:8], refs[8:14], refs[14]
+    far, (keep, give, send), near, sems = refs[:6], refs[6:9], refs[9:15], refs[15]
     copies = fetched(far, near, sems)
     tokens, gain, w_q, w_kv, w_rope, w_out = near
     copies[0].wait()
@@ -86,17 +99,23 @@
     resid = tokens[...].astype(f32)
     scaled = (resid * gain[...].astype(f32)[None, :]).astype(bf16)
     q, kv = w_q.shape[1], w_kv.shape[1]
+    upper = parity() == 1
+    half = resid.shape[0] // 2
+
+    def put(begin, end, value):
+        keep[:, begin:end] = jnp.where(upper, value[half:], value[:half])
+        give[:, begin:end] = jnp.where(upper, value[:half], value[half:])
+
     copies[2].wait()
-    out[:, :q] = dot(scaled, w_q[...])
+    put(0, q, dot(scaled, w_q[...]))
     copies[3].wait()
-    out[:, q : q + kv] = dot(scaled, w_kv[...])
+    put(q, q + kv, dot(scaled, w_kv[...]))
     copies[4].wait()
     tail = dot_t(scaled, w_rope[...])
     square = jnp.sum(resid * resid, axis=1, keepdims=True)
     rest = LANES - tail.shape[1]
-    out[:, q + kv :] = jnp.concatenate(
-        [tail, jnp.broadcast_to(square, (tail.shape[0], rest))], axis=1
-    )
+    tail = jnp.concatenate([tail, jnp.broadcast_to(square, (tail.shape[0], rest))], axis=1)
+    put(q + kv, q + kv + LANES, tail)
     copies[5].wait()
     send[...] = w_out[...].astype(f32)
 
@@ -127,7 +146,8 @@
 
 def attend_kernel(
     heads,
-    sums,
+    own_sums,
+    other_sums,
     gain_q,
     gain_kv,
     cosine,
@@ -153,6 +173,11 @@
     nope = w_key.shape[0] // heads
     vs = w_value.shape[0] // heads
     scale = (nope + rp) ** (-0.5)
+    upper = parity() == 1
+    own, other = own_sums[...], other_sums[...]
+    sums = jnp.concatenate(
+        [jnp.where(upper, other, own), jnp.where(upper, own, other)], axis=0
+    )
     tail = sums[:, qr + kr :]
     inv_in = lax.rsqrt(tail[:, LANES - 1 :] / D + EPS)
     query_latent = normed(inv_in * sums[:, :qr], gain_q[...].astype(f32)[None, :]).astype(bf16)
@@ -229,7 +254,6 @@
             stats = jnp.where(place == i, each, stats)
         mine = groups[half * len(groups) // 2 : (half + 1) * len(groups) // 2]
         halves.append(jnp.concatenate(mine + [stats], axis=1))
-    upper = parity() == 1
     keep[...] = jnp.where(upper, halves[1], halves[0])
     give[...] = jnp.where(upper, halves[0], halves[1])
 
@@ -247,20 +271,23 @@
     return jnp.concatenate(tiles, axis=1)
 
 
-def merge_kernel(in_half, one, two, out):
-    body = one.shape[1] - LANES
-    low = lane((one.shape[0], LANES)) < LANES // 2
-    stats_one, stats_two = one[:, body:], two[:, body:]
-    top = jnp.where(low, jnp.maximum(stats_one, stats_two), 0.0)
-    fade_one = jnp.exp(jnp.where(low, stats_one - top, 0.0))
-    fade_two = jnp.exp(jnp.where(low, stats_two - top, 0.0))
-    total = stats_one * pltpu.roll(fade_one, LANES // 2, 1) + stats_two * pltpu.roll(
-        fade_two, LANES // 2, 1
+def merge_kernel(in_half, *refs):
+    parts, out = refs[:-1], refs[-1]
+    body = out.shape[1] - LANES
+    width = body // in_half
+    low = lane((out.shape[0], LANES)) < LANES // 2
+    stats = [part[:, body:] for part in parts]
+    top = functools.reduce(jnp.maximum, stats)
+    fades = [jnp.exp(jnp.where(low, each - top, 0.0)) for each in stats]
+    total = paired(
+        [each * pltpu.roll(fade, LANES // 2, 1) for each, fade in zip(stats, fades, strict=True)]
     )
     out[:, body:] = jnp.where(low, top, total)
-    width = body // in_half
-    out[:, :body] = one[:, :body] * spread(fade_one, in_half, width) + two[:, :body] * spread(
-        fade_two, in_half, width
+    out[:, :body] = paired(
+        [
+            part[:, :body] * spread(fade, in_half, width)
+            for part, fade in zip(parts, fades, strict=True)
+        ]
     )
 
 
@@ -319,9 +346,9 @@
         for g in range(body // group):
             outs[half * (body // group) + g] = joined[:, g * group : (g + 1) * group]
     me = lax.axis_index("tp")
-    attn = dot(outs[me], w_outs[0][...].astype(bf16))
-    for m in range(1, n_tp):
-        attn += dot(outs[jnp.bitwise_xor(me, m)], w_outs[m][...].astype(bf16))
+    attn = paired(
+        [dot(outs[jnp.bitwise_xor(me, m)], w_outs[m][...].astype(bf16)) for m in range(n_tp)]
+    )
     resid_mid = tokens[...].astype(f32) + attn
     mid[...] = resid_mid
     scaled = (resid_mid * gain[...].astype(f32)[None, :]).astype(bf16)
@@ -384,29 +411,22 @@
     w_out_own = w_attn_out.reshape(-1, d_dev)
 
     first_far = (tokens, gain_in, w_down_q, w_down_kv, w_rope_key.T, w_out_own)
-    sums, w_send = call(
+    sums_half = (n_seq // 2, qr + kr + LANES)
+    keep, give, w_send = call(
         down_kernel,
-        [((n_seq, qr + kr + LANES), f32), (w_out_own.shape, f32)],
+        [(sums_half, f32), (sums_half, f32), (w_out_own.shape, f32)],
         scratch=[pltpu.VMEM(a.shape, a.dtype) for a in first_far]
         + [pltpu.SemaphoreType.DMA((len(first_far),))],
         far=first_far,
     )
     crossed = [bit | 1 for bit in higher_bits("kv", 1)]
     w_outs = [w_out_own]
-    unsent = list(range(1, lax.axis_size("tp")))
-
-    def send(after, count):
-        held, after = lax.optimization_barrier((w_send, after))
-        for m in unsent[:count]:
-            w_outs.append(swap(held, 0, m))
-        del unsent[:count]
-        return after
-
-    for mask in [1] + crossed:
+    w_outs += [swap(w_send, 0, m) for m in range(1, lax.axis_size("tp"))]
+    sums = keep + swap(give, 1)
+    early = sums
+    for i, mask in enumerate(crossed):
         sums = sums + swap(sums, mask)
-        if mask == 1:
-            sums = send(sums, 1)
-        if mask == crossed[0]:
+        if i == 0:
             early = sums
     far = (
         gain_q,
@@ -427,6 +447,8 @@
         scratch=[pltpu.SemaphoreType.DMA((len(far),))],
         far=far,
     )
+    gain_kv, sums = lax.optimization_barrier((gain_kv, sums))
+    other_sums = swap(sums, 1)
     in_half = heads // 2
     state = (n_seq, in_half * vs + LANES)
     new_latent, new_rope, queries, keep, give = call(
@@ -439,6 +461,7 @@
             (state, f32),
         ],
         sums,
+        other_sums,
         gain_q,
         gain_kv,
         cosine,
@@ -464,15 +487,14 @@
         w_value,
     )
 
-    def merge(one, two):
-        return call(functools.partial(merge_kernel, in_half), [(state, f32)], one, two)[0]
+    def merge(*parts):
+        return call(functools.partial(merge_kernel, in_half), [(state, f32)], *parts)[0]
 
     part = merge(keep, swap(give, 1))
     for mask in crossed:
-        part = send(part, 1 if mask == crossed[0] else len(unsent))
         part = merge(part, swap(part, mask))
-    for bit in higher_bits("tp", 0):
-        part = merge(part, swap(part, 1, bit))
+    for masks in tp_rounds():
+        part = merge(part, *[swap(part, bin(m).count("1") % 2, m) for m in masks])
     other = swap(part, 1)
     half = (n_seq, w_ff_in.shape[1] // 2 + LANES)
     resid_mid, keep, give = call(
@@ -491,15 +513,19 @@
     for mask in crossed:
         sums = sums + swap(sums, mask)
     (out,) = call(last_kernel, [((n_seq, d_dev), f32)], sums, swap(sums, 1), w_ff_out)
-    for bit in higher_bits("tp", 0):
-        out = out + swap(out, 0, bit)
+    for masks in tp_rounds():
+        out = paired([out] + [swap(out, 0, m) for m in masks])
     mixed = (resid_mid + out).astype(bf16)
     return (mixed, new_latent, new_rope)
 
 
 def solution(mesh):
+    return sharded(per_device, mesh)
+
+
+def sharded(step, mesh):
     return jax.shard_map(
-        per_device,
+        step,
         mesh=mesh,
         in_specs=(
             P(None, "kv"),

time: 62.7 us -> 62.4 us (level)
  starting transfers between devices: 26.5 us -> 23.4 us
  waiting for transfers between devices: 25.8 us -> 28.1 us
    ppermute x18 -> x21, starting transfers between devices: 26.5 us -> 23.4 us  [swap(): return lax.ppermute(value, BOTH, pairs)]
    ppermute x18 -> x21, waiting for transfers between devices: 25.8 us -> 28.1 us  [swap(): return lax.ppermute(value, BOTH, pairs)]
    pallas_call x11 -> x10, Pallas kernels: 7.33 us -> 7.26 us  [call(): pl.pallas_call(kernel, out_shape=[pltpu.VMEM(s, t) for s, t in outs], in_...]
  transfers between devices with their start and end apart: 18 -> 21, of which waited for: 13 -> 15; matrix products, arithmetic and copies ran while one was open for 2% -> 2% of each run, Pallas kernels for 5% -> 8%
where the time goes in v3:
time: 62.4 us; the launch traced here: 62.2 us
  waiting for transfers between devices  28.1 us (45%)
  starting transfers between devices  23.4 us (38%)
  Pallas kernels  7.26 us (12%)
  local copies, waits for them, and re-layouts  1.79 us (3%)
  between operations  0.79 us (1%)
  other arithmetic  0.78 us (1%)
    ppermute x21, waiting for transfers between devices, swap(): return lax.ppermute(value, BOTH, pairs)  28.1 us
    ppermute x21, starting transfers between devices, swap(): return lax.ppermute(value, BOTH, pairs)  23.4 us
    pallas_call x10, Pallas kernels, call(): pl.pallas_call(kernel, out_shape=[pltpu.VMEM(s, t) for s, t in outs], in_...  7.26 us
    unnamed x14, local copies, waits for them, and re-layouts  1.79 us
  transfers between devices with their start and end apart: 21, of which 15 were waited for; matrix products, arithmetic and copies ran while one was open for 2% of the time, Pallas kernels for 8%

profile of v3, /device:TPU:0, one launch (start us, length us, event | category | flops | bytes accessed | tf_op | source)
XLA Modules:
  0.0 62.2 jit_solution(3517238147206732995)
XLA Ops:
  0.6 1.5 %shard_map.211 = (f32[8,896]{1,0:T(8,128)S(1)}, f32[8,896]{1,0:T(8,128)S(1)}, f32[256,256]{1,0:T(8,128)S(1)}) custom-call(bf16[16,256]{1,0:T(8,128)(2,1)} %refs_9_.1, bf16[256]{0:T(256)(128)(2,1)} %refs_1_.2, bf16[256,512]{1,0:T(8,128)(2,1)} %refs_2_.2, bf16[256,256]{1,0:T(8,128)(2,1)} %refs_3_.1, bf16[32,256]{1,0:T(8,128)(2,1)} %bitcast.22, ...), custom_call_target="tpu_custom_call" | custom-call | tf_op jit(solution)/shard_map/pallas_call | solution.py:58
  2.1 0.6 collective-permute-start
  2.7 0.9 %collective-permute-done = f32[8,896]{1,0:T(8,128)S(1)} collective-permute-done((f32[8,896]{1,0:T(8,128)S(1)}, f32[8,896]{1,0:T(8,128)S(1)}, u32[]{:S(2)}, u32[]{:S(2)}) %collective-permute-start) | collective-permute-done | bytes 28704 | tf_op jit(solution)/shard_map/ppermute | solution.py:26
  3.5 2.7 %collective-permute-start.1 = (f32[8,896]{1,0:T(8,128)S(1)}, f32[8,896]{1,0:T(8,128)S(1)}, u32[]{:S(2)}, u32[]{:S(2)}) collective-permute-start(f32[8,896]{1,0:T(8,128)S(1)} %add.30), channel_id=1, source_target_pairs={{0,12},{1,13},{2,14},{3,15},{4,8},{5,9},{6,10},{7,11},{8,4},{9,5},... | collective-permute-start | bytes 86024 | tf_op jit(solution)/shard_map/ppermute | solution.py:26
  6.2 1.6 %collective-permute-done.1 = f32[8,896]{1,0:T(8,128)S(1)} collective-permute-done((f32[8,896]{1,0:T(8,128)S(1)}, f32[8,896]{1,0:T(8,128)S(1)}, u32[]{:S(2)}, u32[]{:S(2)}) %collective-permute-start.1) | collective-permute-done | bytes 28704 | tf_op jit(solution)/shard_map/ppermute | solution.py:26
  7.8 2.8 %collective-permute-start.2 = (f32[8,896]{1,0:T(8,128)S(1)}, f32[8,896]{1,0:T(8,128)S(1)}, u32[]{:S(2)}, u32[]{:S(2)}) collective-permute-start(f32[8,896]{1,0:T(8,128)S(1)} %add.31.refs_0_), channel_id=1, source_target_pairs={{0,20},{1,21},{2,22},{3,23},{4,16},{5,17},{6,18},{7,19},{8,28},{9,... | collective-permute-start | bytes 86024 | tf_op jit(solution)/shard_map/ppermute | solution.py:26
  10.6 1.5 %collective-permute-start.11 = (f32[256,256]{1,0:T(8,128)S(1)}, f32[256,256]{1,0:T(8,128)S(1)}, u32[]{:S(2)}, u32[]{:S(2)}) collective-permute-start(f32[256,256]{1,0:T(8,128)S(1)} %get-tuple-element.49), channel_id=1, source_target_pairs={{0,1},{1,0},{2,3},{3,2},{4,5},{5,4},{6,7},{7,6},{8,9},{9,8},{10,11... | collective-permute-start | bytes 786440 | tf_op jit(solution)/shard_map/ppermute | solution.py:26
  12.1 1.5 %collective-permute-start.12 = (f32[256,256]{1,0:T(8,128)S(1)}, f32[256,256]{1,0:T(8,128)S(1)}, u32[]{:S(2)}, u32[]{:S(2)}) collective-permute-start(f32[256,256]{1,0:T(8,128)S(1)} %get-tuple-element.49), channel_id=1, source_target_pairs={{0,2},{1,3},{2,0},{3,1},{4,6},{5,7},{6,4},{7,5},{8,10},{9,11},{10,... | collective-permute-start | bytes 786440 | tf_op jit(solution)/shard_map/ppermute | solution.py:26
  13.6 0.5 collective-permute-start.13
  14.1 2.1 %shard_map.212 = (bf16[512]{0:T(512)(128)(2,1)S(1)}, bf16[256]{0:T(256)(128)(2,1)S(1)}, bf16[1024,512]{1,0:T(8,128)(2,1)S(1)}, bf16[512,512]{1,0:T(8,128)(2,1)S(...) custom-call(f32[8,896]{1,0:T(8,128)S(1)} %add.31.refs_0_, ...), custom_call_target="tpu_custom_call" | custom-call | tf_op jit(solution)/shard_map/pallas_call | solution.py:58
  16.3 0.6 copy-done.3
  17.0 0.5 collective-permute-done.3.other_sums
  17.5 1.9 %shard_map.213 = (bf16[16,256]{1,0:T(8,128)(2,1)S(1)}, bf16[16,32]{1,0:T(8,128)(2,1)S(1)}, f32[3,256,128]{2,1,0:T(8,128)S(1)}, f32[16,640]{1,0:T(8,128)S(1)}, f32[16,640]{1,0:T(8,128)S(1)}) custom-call(f32[8,896]{1,0:T(8,128)S(1)} %add.32.own_sums, f32[8,896]{1,0:T(8,128)S(1)} %collective-permute-done.3.other_sums, ...), custom_call_target="tpu_custom_call" | custom-call | tf_op jit(solution)/shard_map/pallas_call | solution.py:58
  19.4 0.2 collective-permute-start.4
  19.6 1.1 %collective-permute-done.4.refs_1_ = f32[16,640]{1,0:T(8,128)S(1)} collective-permute-done((f32[16,640]{1,0:T(8,128)S(1)}, f32[16,640]{1,0:T(8,128)S(1)}, u32[]{:S(2)}, u32[]{:S(2)}) %collective-permute-start.4) | collective-permute-done | bytes 40992 | tf_op jit(solution)/shard_map/ppermute | solution.py:26
  20.6 0.1 shard_map.214.refs_0_
  20.8 1.4 %collective-permute-start.5 = (f32[16,640]{1,0:T(8,128)S(1)}, f32[16,640]{1,0:T(8,128)S(1)}, u32[]{:S(2)}, u32[]{:S(2)}) collective-permute-start(f32[16,640]{1,0:T(8,128)S(1)} %shard_map.214.refs_0_), channel_id=1, source_target_pairs={{0,12},{1,13},{2,14},{3,15},{4,8},{5,9},{6,10},{7,11},{8,4},{9,5},... | collective-permute-start | bytes 122888 | tf_op jit(solution)/shard_map/ppermute | solution.py:26
  22.2 2.2 %collective-permute-done.5.refs_1_ = f32[16,640]{1,0:T(8,128)S(1)} collective-permute-done((f32[16,640]{1,0:T(8,128)S(1)}, f32[16,640]{1,0:T(8,128)S(1)}, u32[]{:S(2)}, u32[]{:S(2)}) %collective-permute-start.5) | collective-permute-done | bytes 40992 | tf_op jit(solution)/shard_map/ppermute | solution.py:26
  24.4 0.1 shard_map.215.refs_0_
  24.5 0.4 collective-permute-start.6
  24.9 4.0 %collective-permute-done.6.refs_1_ = f32[16,640]{1,0:T(8,128)S(1)} collective-permute-done((f32[16,640]{1,0:T(8,128)S(1)}, f32[16,640]{1,0:T(8,128)S(1)}, u32[]{:S(2)}, u32[]{:S(2)}) %collective-permute-start.6) | collective-permute-done | bytes 40992 | tf_op jit(solution)/shard_map/ppermute | solution.py:26
  28.9 0.1 shard_map.216.refs_0_
  29.0 1.6 %collective-permute-start.7 = (f32[16,640]{1,0:T(8,128)S(1)}, f32[16,640]{1,0:T(8,128)S(1)}, u32[]{:S(2)}, u32[]{:S(2)}) collective-permute-start(f32[16,640]{1,0:T(8,128)S(1)} %shard_map.216.refs_0_), channel_id=1, source_target_pairs={{0,5},{1,4},{2,7},{3,6},{4,1},{5,0},{6,3},{7,2},{8,13},{9,12},{10,... | collective-permute-start | bytes 122888 | tf_op jit(solution)/shard_map/ppermute | solution.py:26
  30.7 1.2 %collective-permute-start.8 = (f32[16,640]{1,0:T(8,128)S(1)}, f32[16,640]{1,0:T(8,128)S(1)}, u32[]{:S(2)}, u32[]{:S(2)}) collective-permute-start(f32[16,640]{1,0:T(8,128)S(1)} %shard_map.216.refs_0_), channel_id=1, source_target_pairs={{0,6},{1,7},{2,4},{3,5},{4,2},{5,3},{6,0},{7,1},{8,14},{9,15},{10,... | collective-permute-start | bytes 122888 | tf_op jit(solution)/shard_map/ppermute | solution.py:26
  31.8 0.7 %collective-permute-done.7.refs_1_ = f32[16,640]{1,0:T(8,128)S(1)} collective-permute-done((f32[16,640]{1,0:T(8,128)S(1)}, f32[16,640]{1,0:T(8,128)S(1)}, u32[]{:S(2)}, u32[]{:S(2)}) %collective-permute-start.7) | collective-permute-done | bytes 40992 | tf_op jit(solution)/shard_map/ppermute | solution.py:26
  32.5 2.4 %collective-permute-start.9 = (f32[16,640]{1,0:T(8,128)S(1)}, f32[16,640]{1,0:T(8,128)S(1)}, u32[]{:S(2)}, u32[]{:S(2)}) collective-permute-start(f32[16,640]{1,0:T(8,128)S(1)} %shard_map.216.refs_0_), channel_id=1, source_target_pairs={{0,3},{1,2},{2,1},{3,0},{4,7},{5,6},{6,5},{7,4},{8,11},{9,10},{10,... | collective-permute-start | bytes 122888 | tf_op jit(solution)/shard_map/ppermute | solution.py:26
  35.0 2.5 %collective-permute-done.9.refs_3_ = f32[16,640]{1,0:T(8,128)S(1)} collective-permute-done((f32[16,640]{1,0:T(8,128)S(1)}, f32[16,640]{1,0:T(8,128)S(1)}, u32[]{:S(2)}, u32[]{:S(2)}) %collective-permute-start.9) | collective-permute-done | bytes 40992 | tf_op jit(solution)/shard_map/ppermute | solution.py:26
  37.5 0.2 shard_map.217.refs_0_
  37.8 0.3 shard_map.218
  38.0 0.9 %collective-permute-done.10.refs_1_ = f32[16,640]{1,0:T(8,128)S(1)} collective-permute-done((f32[16,640]{1,0:T(8,128)S(1)}, f32[16,640]{1,0:T(8,128)S(1)}, u32[]{:S(2)}, u32[]{:S(2)}) %collective-permute-start.10) | collective-permute-done | bytes 40992 | tf_op jit(solution)/shard_map/ppermute | solution.py:26
  39.0 0.7 %shard_map.219 = (f32[16,256]{1,0:T(8,128)S(1)}, f32[16,1152]{1,0:T(8,128)S(1)}, f32[16,1152]{1,0:T(8,128)S(1)}) custom-call(f32[16,640]{1,0:T(8,128)S(1)} %shard_map.217.refs_0_, f32[16,640]{1,0:T(8,128)S(1)} %collective-permute-done.10.refs_1_, f32[2,16,128]{2,1,0:T(8,128)S(1)} %get-tuple-element.45.refs_2_, f32[16,1024]{1,0:T(8,128)S(1)} %get-tuple-element.46.refs_3_, ...), custom_call_target="tpu_custom_call" | custom-call | tf_op jit(solution)/shard_map/pallas_call | solution.py:58
  39.7 0.2 collective-permute-start.14
  39.9 1.1 %collective-permute-done.14 = f32[16,1152]{1,0:T(8,128)S(1)} collective-permute-done((f32[16,1152]{1,0:T(8,128)S(1)}, f32[16,1152]{1,0:T(8,128)S(1)}, u32[]{:S(2)}, u32[]{:S(2)}) %collective-permute-start.14) | collective-permute-done | bytes 73760 | tf_op jit(solution)/shard_map/ppermute | solution.py:26
  41.0 1.4 %collective-permute-start.15 = (f32[16,1152]{1,0:T(8,128)S(1)}, f32[16,1152]{1,0:T(8,128)S(1)}, u32[]{:S(2)}, u32[]{:S(2)}) collective-permute-start(f32[16,1152]{1,0:T(8,128)S(1)} %add.33), channel_id=1, source_target_pairs={{0,12},{1,13},{2,14},{3,15},{4,8},{5,9},{6,10},{7,11},{8,4},{9,5},... | collective-permute-start | bytes 221192 | tf_op jit(solution)/shard_map/ppermute | solution.py:26
  42.5 2.8 %collective-permute-done.15 = f32[16,1152]{1,0:T(8,128)S(1)} collective-permute-done((f32[16,1152]{1,0:T(8,128)S(1)}, f32[16,1152]{1,0:T(8,128)S(1)}, u32[]{:S(2)}, u32[]{:S(2)}) %collective-permute-start.15) | collective-permute-done | bytes 73760 | tf_op jit(solution)/shard_map/ppermute | solution.py:26
  45.3 1.0 %collective-permute-start.16 = (f32[16,1152]{1,0:T(8,128)S(1)}, f32[16,1152]{1,0:T(8,128)S(1)}, u32[]{:S(2)}, u32[]{:S(2)}) collective-permute-start(f32[16,1152]{1,0:T(8,128)S(1)} %add.34), channel_id=1, source_target_pairs={{0,20},{1,21},{2,22},{3,23},{4,16},{5,17},{6,18},{7,19},{8,28},{9,... | collective-permute-start | bytes 221192 | tf_op jit(solution)/shard_map/ppermute | solution.py:26
  46.3 5.8 %collective-permute-done.16 = f32[16,1152]{1,0:T(8,128)S(1)} collective-permute-done((f32[16,1152]{1,0:T(8,128)S(1)}, f32[16,1152]{1,0:T(8,128)S(1)}, u32[]{:S(2)}, u32[]{:S(2)}) %collective-permute-start.16) | collective-permute-done | bytes 73760 | tf_op jit(solution)/shard_map/ppermute | solution.py:26
  52.1 0.2 collective-permute-start.17
  52.3 1.1 %collective-permute-done.17.other = f32[16,1152]{1,0:T(8,128)S(1)} collective-permute-done((f32[16,1152]{1,0:T(8,128)S(1)}, f32[16,1152]{1,0:T(8,128)S(1)}, u32[]{:S(2)}, u32[]{:S(2)}) %collective-permute-start.17) | collective-permute-done | bytes 73760 | tf_op jit(solution)/shard_map/ppermute | solution.py:26
  53.4 0.3 shard_map.220
  53.7 1.7 %collective-permute-start.18 = (f32[16,256]{1,0:T(8,128)S(1)}, f32[16,256]{1,0:T(8,128)S(1)}, u32[]{:S(2)}, u32[]{:S(2)}) collective-permute-start(f32[16,256]{1,0:T(8,128)S(1)} %shard_map.220), channel_id=1, source_target_pairs={{0,1},{1,0},{2,3},{3,2},{4,5},{5,4},{6,7},{7,6},{8,9},{9,8},{10,11... | collective-permute-start | bytes 49160 | tf_op jit(solution)/shard_map/ppermute | solution.py:26
  55.4 1.5 %collective-permute-start.19 = (f32[16,256]{1,0:T(8,128)S(1)}, f32[16,256]{1,0:T(8,128)S(1)}, u32[]{:S(2)}, u32[]{:S(2)}) collective-permute-start(f32[16,256]{1,0:T(8,128)S(1)} %shard_map.220), channel_id=1, source_target_pairs={{0,2},{1,3},{2,0},{3,1},{4,6},{5,7},{6,4},{7,5},{8,10},{9,11},{10,... | collective-permute-start | bytes 49160 | tf_op jit(solution)/shard_map/ppermute | solution.py:26
  56.9 0.3 collective-permute-start.20
  57.2 0.6 copy.23
  57.8 0.6 copy.24
  58.4 0.7 %collective-permute-done.19 = f32[16,256]{1,0:T(8,128)S(1)} collective-permute-done((f32[16,256]{1,0:T(8,128)S(1)}, f32[16,256]{1,0:T(8,128)S(1)}, u32[]{:S(2)}, u32[]{:S(2)}) %collective-permute-start.19) | collective-permute-done | bytes 16416 | tf_op jit(solution)/shard_map/ppermute | solution.py:26
  59.1 2.4 %collective-permute-done.20 = f32[16,256]{1,0:T(8,128)S(1)} collective-permute-done((f32[16,256]{1,0:T(8,128)S(1)}, f32[16,256]{1,0:T(8,128)S(1)}, u32[]{:S(2)}, u32[]{:S(2)}) %collective-permute-start.20) | collective-permute-done | bytes 16416 | tf_op jit(solution)/shard_map/ppermute | solution.py:26
  61.5 0.6 add_convert_fusion
  (27 shorter events, 0.4 us)
Async XLA Ops:
  2.1 1.4 %collective-permute-start = (f32[8,896]{1,0:T(8,128)S(1)}, f32[8,896]{1,0:T(8,128)S(1)}, u32[]{:S(2)}, u32[]{:S(2)}) collective-permute-start(f32[8,896]{1,0:T(8,128)S(1)} %get-tuple-element.29), channel_id=1, source_target_pairs={{0,4},{1,5},{2,6},{3,7},{4,0},{5,1},{6,2},{7,3},{8,12},{9,13},{10,... | collective-permute-start | bytes 86024 | tf_op jit(solution)/shard_map/ppermute | solution.py:26
  3.5 4.2 %collective-permute-start.1 = (f32[8,896]{1,0:T(8,128)S(1)}, f32[8,896]{1,0:T(8,128)S(1)}, u32[]{:S(2)}, u32[]{:S(2)}) collective-permute-start(f32[8,896]{1,0:T(8,128)S(1)} %add.30), channel_id=1, source_target_pairs={{0,12},{1,13},{2,14},{3,15},{4,8},{5,9},{6,10},{7,11},{8,4},{9,5},... | collective-permute-start | bytes 86024 | tf_op jit(solution)/shard_map/ppermute | solution.py:26
  7.8 6.3 %copy-start.5 = (s32[16]{0:T(128)S(1)}, s32[16]{0:T(128)}, u32[]{:S(2)}) copy-start(s32[16]{0:T(128)} %param.21) | copy-start | bytes 196
  7.8 8.4 %collective-permute-start.2 = (f32[8,896]{1,0:T(8,128)S(1)}, f32[8,896]{1,0:T(8,128)S(1)}, u32[]{:S(2)}, u32[]{:S(2)}) collective-permute-start(f32[8,896]{1,0:T(8,128)S(1)} %add.31.refs_0_), channel_id=1, source_target_pairs={{0,20},{1,21},{2,22},{3,23},{4,16},{5,17},{6,18},{7,19},{8,28},{9,... | collective-permute-start | bytes 86024 | tf_op jit(solution)/shard_map/ppermute | solution.py:26
  10.6 27.4 %collective-permute-start.11 = (f32[256,256]{1,0:T(8,128)S(1)}, f32[256,256]{1,0:T(8,128)S(1)}, u32[]{:S(2)}, u32[]{:S(2)}) collective-permute-start(f32[256,256]{1,0:T(8,128)S(1)} %get-tuple-element.49), channel_id=1, source_target_pairs={{0,1},{1,0},{2,3},{3,2},{4,5},{5,4},{6,7},{7,6},{8,9},{9,8},{10,11... | collective-permute-start | bytes 786440 | tf_op jit(solution)/shard_map/ppermute | solution.py:26
  12.1 25.9 %collective-permute-start.12 = (f32[256,256]{1,0:T(8,128)S(1)}, f32[256,256]{1,0:T(8,128)S(1)}, u32[]{:S(2)}, u32[]{:S(2)}) collective-permute-start(f32[256,256]{1,0:T(8,128)S(1)} %get-tuple-element.49), channel_id=1, source_target_pairs={{0,2},{1,3},{2,0},{3,1},{4,6},{5,7},{6,4},{7,5},{8,10},{9,11},{10,... | collective-permute-start | bytes 786440 | tf_op jit(solution)/shard_map/ppermute | solution.py:26
  13.6 24.4 %collective-permute-start.13 = (f32[256,256]{1,0:T(8,128)S(1)}, f32[256,256]{1,0:T(8,128)S(1)}, u32[]{:S(2)}, u32[]{:S(2)}) collective-permute-start(f32[256,256]{1,0:T(8,128)S(1)} %get-tuple-element.49), channel_id=1, source_target_pairs={{0,3},{1,2},{2,1},{3,0},{4,7},{5,6},{6,5},{7,4},{8,11},{9,10},{10,... | collective-permute-start | bytes 786440 | tf_op jit(solution)/shard_map/ppermute | solution.py:26
  16.2 0.7 %copy-start.3 = (f32[128]{0:T(128)S(1)}, f32[128]{0:T(128)}, u32[]{:S(2)}) copy-start(f32[128]{0:T(128)} %constant.5.clone) | copy-start | bytes 1540
  16.2 0.7 %copy-start.4 = (f32[128]{0:T(128)S(1)}, f32[128]{0:T(128)}, u32[]{:S(2)}) copy-start(f32[128]{0:T(128)} %constant.6) | copy-start | bytes 1540
  16.2 1.3 %collective-permute-start.3 = (f32[8,896]{1,0:T(8,128)S(1)}, f32[8,896]{1,0:T(8,128)S(1)}, u32[]{:S(2)}, u32[]{:S(2)}) collective-permute-start(f32[8,896]{1,0:T(8,128)S(1)} %add.32.own_sums), channel_id=1, source_target_pairs={{0,4},{1,5},{2,6},{3,7},{4,0},{5,1},{6,2},{7,3},{8,12},{9,13},{10,... | collective-permute-start | bytes 86024 | tf_op jit(solution)/shard_map/ppermute | solution.py:26
  19.3 19.6 %copy-start = (bf16[256,2048]{1,0:T(8,128)(2,1)S(1)}, bf16[256,2048]{1,0:T(8,128)(2,1)}, u32[]{:S(2)}) copy-start(bf16[256,2048]{1,0:T(8,128)(2,1)} %refs_6_.1) | copy-start | bytes 3145732
  19.4 1.3 %collective-permute-start.4 = (f32[16,640]{1,0:T(8,128)S(1)}, f32[16,640]{1,0:T(8,128)S(1)}, u32[]{:S(2)}, u32[]{:S(2)}) collective-permute-start(f32[16,640]{1,0:T(8,128)S(1)} %get-tuple-element.41), channel_id=1, source_target_pairs={{0,4},{1,5},{2,6},{3,7},{4,0},{5,1},{6,2},{7,3},{8,12},{9,13},{10,... | collective-permute-start | bytes 122888 | tf_op jit(solution)/shard_map/ppermute | solution.py:26
  20.8 3.6 %collective-permute-start.5 = (f32[16,640]{1,0:T(8,128)S(1)}, f32[16,640]{1,0:T(8,128)S(1)}, u32[]{:S(2)}, u32[]{:S(2)}) collective-permute-start(f32[16,640]{1,0:T(8,128)S(1)} %shard_map.214.refs_0_), channel_id=1, source_target_pairs={{0,12},{1,13},{2,14},{3,15},{4,8},{5,9},{6,10},{7,11},{8,4},{9,5},... | collective-permute-start | bytes 122888 | tf_op jit(solution)/shard_map/ppermute | solution.py:26
  24.5 4.4 %collective-permute-start.6 = (f32[16,640]{1,0:T(8,128)S(1)}, f32[16,640]{1,0:T(8,128)S(1)}, u32[]{:S(2)}, u32[]{:S(2)}) collective-permute-start(f32[16,640]{1,0:T(8,128)S(1)} %shard_map.215.refs_0_), channel_id=1, source_target_pairs={{0,20},{1,21},{2,22},{3,23},{4,16},{5,17},{6,18},{7,19},{8,28},{9,... | collective-permute-start | bytes 122888 | tf_op jit(solution)/shard_map/ppermute | solution.py:26
  29.0 3.5 %collective-permute-start.7 = (f32[16,640]{1,0:T(8,128)S(1)}, f32[16,640]{1,0:T(8,128)S(1)}, u32[]{:S(2)}, u32[]{:S(2)}) collective-permute-start(f32[16,640]{1,0:T(8,128)S(1)} %shard_map.216.refs_0_), channel_id=1, source_target_pairs={{0,5},{1,4},{2,7},{3,6},{4,1},{5,0},{6,3},{7,2},{8,13},{9,12},{10,... | collective-permute-start | bytes 122888 | tf_op jit(solution)/shard_map/ppermute | solution.py:26
  30.7 4.3 %collective-permute-start.8 = (f32[16,640]{1,0:T(8,128)S(1)}, f32[16,640]{1,0:T(8,128)S(1)}, u32[]{:S(2)}, u32[]{:S(2)}) collective-permute-start(f32[16,640]{1,0:T(8,128)S(1)} %shard_map.216.refs_0_), channel_id=1, source_target_pairs={{0,6},{1,7},{2,4},{3,5},{4,2},{5,3},{6,0},{7,1},{8,14},{9,15},{10,... | collective-permute-start | bytes 122888 | tf_op jit(solution)/shard_map/ppermute | solution.py:26
  32.5 4.9 %collective-permute-start.9 = (f32[16,640]{1,0:T(8,128)S(1)}, f32[16,640]{1,0:T(8,128)S(1)}, u32[]{:S(2)}, u32[]{:S(2)}) collective-permute-start(f32[16,640]{1,0:T(8,128)S(1)} %shard_map.216.refs_0_), channel_id=1, source_target_pairs={{0,3},{1,2},{2,1},{3,0},{4,7},{5,6},{6,5},{7,4},{8,11},{9,10},{10,... | collective-permute-start | bytes 122888 | tf_op jit(solution)/shard_map/ppermute | solution.py:26
  37.7 1.3 %collective-permute-start.10 = (f32[16,640]{1,0:T(8,128)S(1)}, f32[16,640]{1,0:T(8,128)S(1)}, u32[]{:S(2)}, u32[]{:S(2)}) collective-permute-start(f32[16,640]{1,0:T(8,128)S(1)} %shard_map.217.refs_0_), channel_id=1, source_target_pairs={{0,4},{1,5},{2,6},{3,7},{4,0},{5,1},{6,2},{7,3},{8,12},{9,13},{10,... | collective-permute-start | bytes 122888 | tf_op jit(solution)/shard_map/ppermute | solution.py:26
  37.7 1.2 %copy-start.2 = (bf16[4,64,256]{2,1,0:T(8,128)(2,1)S(1)}, bf16[4,64,256]{2,1,0:T(8,128)(2,1)}, u32[]{:S(2)}) copy-start(bf16[4,64,256]{2,1,0:T(8,128)(2,1)} %param.34) | copy-start | bytes 393220
  39.0 14.5 %copy-start.1 = (bf16[2048,256]{1,0:T(8,128)(2,1)S(1)}, bf16[2048,256]{1,0:T(8,128)(2,1)}, u32[]{:S(2)}) copy-start(bf16[2048,256]{1,0:T(8,128)(2,1)} %w_out.1) | copy-start | bytes 3145732
  39.7 1.3 %collective-permute-start.14 = (f32[16,1152]{1,0:T(8,128)S(1)}, f32[16,1152]{1,0:T(8,128)S(1)}, u32[]{:S(2)}, u32[]{:S(2)}) collective-permute-start(f32[16,1152]{1,0:T(8,128)S(1)} %get-tuple-element.52), channel_id=1, source_target_pairs={{0,4},{1,5},{2,6},{3,7},{4,0},{5,1},{6,2},{7,3},{8,12},{9,13},{10,... | collective-permute-start | bytes 221192 | tf_op jit(solution)/shard_map/ppermute | solution.py:26
  41.0 4.3 %collective-permute-start.15 = (f32[16,1152]{1,0:T(8,128)S(1)}, f32[16,1152]{1,0:T(8,128)S(1)}, u32[]{:S(2)}, u32[]{:S(2)}) collective-permute-start(f32[16,1152]{1,0:T(8,128)S(1)} %add.33), channel_id=1, source_target_pairs={{0,12},{1,13},{2,14},{3,15},{4,8},{5,9},{6,10},{7,11},{8,4},{9,5},... | collective-permute-start | bytes 221192 | tf_op jit(solution)/shard_map/ppermute | solution.py:26
  45.3 6.8 %collective-permute-start.16 = (f32[16,1152]{1,0:T(8,128)S(1)}, f32[16,1152]{1,0:T(8,128)S(1)}, u32[]{:S(2)}, u32[]{:S(2)}) collective-permute-start(f32[16,1152]{1,0:T(8,128)S(1)} %add.34), channel_id=1, source_target_pairs={{0,20},{1,21},{2,22},{3,23},{4,16},{5,17},{6,18},{7,19},{8,28},{9,... | collective-permute-start | bytes 221192 | tf_op jit(solution)/shard_map/ppermute | solution.py:26
  52.1 1.3 %collective-permute-start.17 = (f32[16,1152]{1,0:T(8,128)S(1)}, f32[16,1152]{1,0:T(8,128)S(1)}, u32[]{:S(2)}, u32[]{:S(2)}) collective-permute-start(f32[16,1152]{1,0:T(8,128)S(1)} %add.35.own), channel_id=1, source_target_pairs={{0,4},{1,5},{2,6},{3,7},{4,0},{5,1},{6,2},{7,3},{8,12},{9,13},{10,... | collective-permute-start | bytes 221192 | tf_op jit(solution)/shard_map/ppermute | solution.py:26
  53.7 4.7 %collective-permute-start.18 = (f32[16,256]{1,0:T(8,128)S(1)}, f32[16,256]{1,0:T(8,128)S(1)}, u32[]{:S(2)}, u32[]{:S(2)}) collective-permute-start(f32[16,256]{1,0:T(8,128)S(1)} %shard_map.220), channel_id=1, source_target_pairs={{0,1},{1,0},{2,3},{3,2},{4,5},{5,4},{6,7},{7,6},{8,9},{9,8},{10,11... | collective-permute-start | bytes 49160 | tf_op jit(solution)/shard_map/ppermute | solution.py:26
  55.4 3.7 %collective-permute-start.19 = (f32[16,256]{1,0:T(8,128)S(1)}, f32[16,256]{1,0:T(8,128)S(1)}, u32[]{:S(2)}, u32[]{:S(2)}) collective-permute-start(f32[16,256]{1,0:T(8,128)S(1)} %shard_map.220), channel_id=1, source_target_pairs={{0,2},{1,3},{2,0},{3,1},{4,6},{5,7},{6,4},{7,5},{8,10},{9,11},{10,... | collective-permute-start | bytes 49160 | tf_op jit(solution)/shard_map/ppermute | solution.py:26
  56.9 4.6 %collective-permute-start.20 = (f32[16,256]{1,0:T(8,128)S(1)}, f32[16,256]{1,0:T(8,128)S(1)}, u32[]{:S(2)}, u32[]{:S(2)}) collective-permute-start(f32[16,256]{1,0:T(8,128)S(1)} %shard_map.220), channel_id=1, source_target_pairs={{0,3},{1,2},{2,1},{3,0},{4,7},{5,6},{6,5},{7,4},{8,11},{9,10},{10,... | collective-permute-start | bytes 49160 | tf_op jit(solution)/shard_map/ppermute | solution.py:26

commit v4 on v3

--- a/solution.py
+++ b/solution.py
@@ -38,10 +38,14 @@
     return terms[0]
 
 
-def tp_rounds():
-    found = higher_bits("tp", 0)
+def rounds(axis, first):
+    found = higher_bits(axis, first)
     pairs = [found[i : i + 2] for i in range(0, len(found), 2)]
     return [pair + [sum(pair)] if len(pair) == 2 else pair for pair in pairs]
+
+
+def crossing(mask):
+    return mask.bit_count() % 2
 
 
 def parity():
@@ -352,22 +356,34 @@
     resid_mid = tokens[...].astype(f32) + attn
     mid[...] = resid_mid
     scaled = (resid_mid * gain[...].astype(f32)[None, :]).astype(bf16)
-    square = jnp.broadcast_to(jnp.sum(resid_mid * resid_mid, axis=1, keepdims=True), (n_seq, LANES))
+    square = jnp.sum(resid_mid * resid_mid, axis=1, keepdims=True)
     hidden = dot(scaled, w_in[...])
     half = hidden.shape[1] // 2
-    keep[:, :half] = jnp.where(upper, hidden[:, half:], hidden[:, :half])
-    give[:, :half] = jnp.where(upper, hidden[:, :half], hidden[:, half:])
-    keep[:, half:] = square
-    give[:, half:] = square
+    for i in range(half // LANES):
+        one = hidden[:, i * LANES : (i + 1) * LANES]
+        two = hidden[:, half + i * LANES : half + (i + 1) * LANES]
+        keep[i * n_seq : (i + 1) * n_seq, :] = jnp.where(upper, two, one)
+        give[i * n_seq : (i + 1) * n_seq, :] = jnp.where(upper, one, two)
+    few = n_seq // 2
+    squares = jnp.where(lane((few, LANES)) < LANES // 2, square[:few], square[few:])
+    keep[half // LANES * n_seq :, :] = squares
+    give[half // LANES * n_seq :, :] = squares
 
 
 def last_kernel(own, other, w_out, out):
-    half = own.shape[1] - LANES
-    inv_mid = lax.rsqrt(own[:, half : half + 1] / D + EPS)
+    n_seq = out.shape[0]
+    tiles = own.shape[0] // n_seq
+    half = tiles * LANES
+    squares = own[tiles * n_seq :, :]
+    square = jnp.concatenate([squares[:, :1], squares[:, LANES // 2 : LANES // 2 + 1]], axis=0)
+    inv_mid = lax.rsqrt(square / D + EPS)
     mine = parity()
     total = None
     for part, place in ((own, mine), (other, 1 - mine)):
-        hidden = jnp.square(jax.nn.relu(inv_mid * part[:, :half])).astype(bf16)
+        hidden = jnp.concatenate(
+            [part[i * n_seq : (i + 1) * n_seq, :] for i in range(tiles)], axis=1
+        )
+        hidden = jnp.square(jax.nn.relu(inv_mid * hidden)).astype(bf16)
         begin = pl.multiple_of(place * half, half)
         term = dot(hidden, w_out[pl.ds(begin, half), :])
         total = term if total is None else total + term
@@ -419,14 +435,14 @@
         + [pltpu.SemaphoreType.DMA((len(first_far),))],
         far=first_far,
     )
-    crossed = [bit | 1 for bit in higher_bits("kv", 1)]
+    kv_rounds, tp_rounds = rounds("kv", 1), rounds("tp", 0)
     w_outs = [w_out_own]
     w_outs += [swap(w_send, 0, m) for m in range(1, lax.axis_size("tp"))]
     sums = keep + swap(give, 1)
     early = sums
-    for i, mask in enumerate(crossed):
-        sums = sums + swap(sums, mask)
-        if i == 0:
+    for bit in higher_bits("kv", 1):
+        sums = sums + swap(sums, bit | 1)
+        if bit == 2:
             early = sums
     far = (
         gain_q,
@@ -491,12 +507,12 @@
         return call(functools.partial(merge_kernel, in_half), [(state, f32)], *parts)[0]
 
     part = merge(keep, swap(give, 1))
-    for mask in crossed:
-        part = merge(part, swap(part, mask))
-    for masks in tp_rounds():
-        part = merge(part, *[swap(part, bin(m).count("1") % 2, m) for m in masks])
+    for masks in kv_rounds:
+        part = merge(part, *[swap(part, m | crossing(m)) for m in masks])
+    for masks in tp_rounds:
+        part = merge(part, *[swap(part, crossing(m), m) for m in masks])
     other = swap(part, 1)
-    half = (n_seq, w_ff_in.shape[1] // 2 + LANES)
+    half = (w_ff_in.shape[1] // 2 // LANES * n_seq + n_seq // 2, LANES)
     resid_mid, keep, give = call(
         functools.partial(middle_kernel, heads),
         [((n_seq, d_dev), f32), (half, f32), (half, f32)],
@@ -510,10 +526,10 @@
         scratch=[pltpu.VMEM((lax.axis_size("tp"), n_seq, w_out_own.shape[0]), bf16)],
     )
     sums = keep + swap(give, 1)
-    for mask in crossed:
-        sums = sums + swap(sums, mask)
+    for masks in kv_rounds:
+        sums = paired([sums] + [swap(sums, m | crossing(m)) for m in masks])
     (out,) = call(last_kernel, [((n_seq, d_dev), f32)], sums, swap(sums, 1), w_ff_out)
-    for masks in tp_rounds():
+    for masks in tp_rounds:
         out = paired([out] + [swap(out, 0, m) for m in masks])
     mixed = (resid_mid + out).astype(bf16)
     return (mixed, new_latent, new_rope)

time: 62.4 us -> 62 us (level)
  waiting for transfers between devices: 28.1 us -> 26.8 us
  starting transfers between devices: 23.4 us -> 24.4 us
    ppermute x21 -> x23, waiting for transfers between devices: 28.1 us -> 26.8 us  [swap(): return lax.ppermute(value, BOTH, pairs)]
    ppermute x21 -> x23, starting transfers between devices: 23.4 us -> 24.4 us  [swap(): return lax.ppermute(value, BOTH, pairs)]
    pallas_call x10 -> x9, Pallas kernels: 7.26 us -> 7.25 us  [call(): pl.pallas_call(kernel, out_shape=[pltpu.VMEM(s, t) for s, t in outs], in_...]
  transfers between devices with their start and end apart: 21 -> 23, of which waited for: 15 -> 16; matrix products, arithmetic and copies ran while one was open for 2% -> 2% of each run, Pallas kernels for 8% -> 8%
where the time goes in v4:
time: 62 us; the launch traced here: 61.8 us
  waiting for transfers between devices  26.8 us (43%)
  starting transfers between devices  24.4 us (39%)
  Pallas kernels  7.25 us (12%)
  local copies, waits for them, and re-layouts  1.79 us (3%)
  other arithmetic  0.77 us (1%)
  between operations  0.77 us (1%)
    ppermute x23, waiting for transfers between devices, swap(): return lax.ppermute(value, BOTH, pairs)  26.8 us
    ppermute x23, starting transfers between devices, swap(): return lax.ppermute(value, BOTH, pairs)  24.4 us
    pallas_call x9, Pallas kernels, call(): pl.pallas_call(kernel, out_shape=[pltpu.VMEM(s, t) for s, t in outs], in_...  7.25 us
    unnamed x14, local copies, waits for them, and re-layouts  1.79 us
  transfers between devices with their start and end apart: 23, of which 16 were waited for; matrix products, arithmetic and copies ran while one was open for 2% of the time, Pallas kernels for 8%

profile of v4, /device:TPU:0, one launch (start us, length us, event | category | flops | bytes accessed | tf_op | source)
XLA Modules:
  0.0 61.8 jit_solution(3920793947731455536)
XLA Ops:
  0.6 1.5 %shard_map.211 = (f32[8,896]{1,0:T(8,128)S(1)}, f32[8,896]{1,0:T(8,128)S(1)}, f32[256,256]{1,0:T(8,128)S(1)}) custom-call(bf16[16,256]{1,0:T(8,128)(2,1)} %refs_9_.1, bf16[256]{0:T(256)(128)(2,1)} %refs_1_.2, bf16[256,512]{1,0:T(8,128)(2,1)} %refs_2_.2, bf16[256,256]{1,0:T(8,128)(2,1)} %refs_3_.1, bf16[32,256]{1,0:T(8,128)(2,1)} %bitcast.22, ...), custom_call_target="tpu_custom_call" | custom-call | tf_op jit(solution)/shard_map/pallas_call | solution.py:62
  2.1 0.6 collective-permute-start
  2.7 0.9 %collective-permute-done = f32[8,896]{1,0:T(8,128)S(1)} collective-permute-done((f32[8,896]{1,0:T(8,128)S(1)}, f32[8,896]{1,0:T(8,128)S(1)}, u32[]{:S(2)}, u32[]{:S(2)}) %collective-permute-start) | collective-permute-done | bytes 28704 | tf_op jit(solution)/shard_map/ppermute | solution.py:26
  3.5 2.7 %collective-permute-start.1 = (f32[8,896]{1,0:T(8,128)S(1)}, f32[8,896]{1,0:T(8,128)S(1)}, u32[]{:S(2)}, u32[]{:S(2)}) collective-permute-start(f32[8,896]{1,0:T(8,128)S(1)} %add.33), channel_id=1, source_target_pairs={{0,12},{1,13},{2,14},{3,15},{4,8},{5,9},{6,10},{7,11},{8,4},{9,5},... | collective-permute-start | bytes 86024 | tf_op jit(solution)/shard_map/ppermute | solution.py:26
  6.2 1.6 %collective-permute-done.1 = f32[8,896]{1,0:T(8,128)S(1)} collective-permute-done((f32[8,896]{1,0:T(8,128)S(1)}, f32[8,896]{1,0:T(8,128)S(1)}, u32[]{:S(2)}, u32[]{:S(2)}) %collective-permute-start.1) | collective-permute-done | bytes 28704 | tf_op jit(solution)/shard_map/ppermute | solution.py:26
  7.8 2.8 %collective-permute-start.2 = (f32[8,896]{1,0:T(8,128)S(1)}, f32[8,896]{1,0:T(8,128)S(1)}, u32[]{:S(2)}, u32[]{:S(2)}) collective-permute-start(f32[8,896]{1,0:T(8,128)S(1)} %add.34.refs_0_), channel_id=1, source_target_pairs={{0,20},{1,21},{2,22},{3,23},{4,16},{5,17},{6,18},{7,19},{8,28},{9,... | collective-permute-start | bytes 86024 | tf_op jit(solution)/shard_map/ppermute | solution.py:26
  10.6 1.5 %collective-permute-start.12 = (f32[256,256]{1,0:T(8,128)S(1)}, f32[256,256]{1,0:T(8,128)S(1)}, u32[]{:S(2)}, u32[]{:S(2)}) collective-permute-start(f32[256,256]{1,0:T(8,128)S(1)} %get-tuple-element.49), channel_id=1, source_target_pairs={{0,1},{1,0},{2,3},{3,2},{4,5},{5,4},{6,7},{7,6},{8,9},{9,8},{10,11... | collective-permute-start | bytes 786440 | tf_op jit(solution)/shard_map/ppermute | solution.py:26
  12.1 1.5 %collective-permute-start.13 = (f32[256,256]{1,0:T(8,128)S(1)}, f32[256,256]{1,0:T(8,128)S(1)}, u32[]{:S(2)}, u32[]{:S(2)}) collective-permute-start(f32[256,256]{1,0:T(8,128)S(1)} %get-tuple-element.49), channel_id=1, source_target_pairs={{0,2},{1,3},{2,0},{3,1},{4,6},{5,7},{6,4},{7,5},{8,10},{9,11},{10,... | collective-permute-start | bytes 786440 | tf_op jit(solution)/shard_map/ppermute | solution.py:26
  13.6 0.5 collective-permute-start.14
  14.1 2.1 %shard_map.212 = (bf16[512]{0:T(512)(128)(2,1)S(1)}, bf16[256]{0:T(256)(128)(2,1)S(1)}, bf16[1024,512]{1,0:T(8,128)(2,1)S(1)}, bf16[512,512]{1,0:T(8,128)(2,1)S(...) custom-call(f32[8,896]{1,0:T(8,128)S(1)} %add.34.refs_0_, ...), custom_call_target="tpu_custom_call" | custom-call | tf_op jit(solution)/shard_map/pallas_call | solution.py:62
  16.3 0.6 copy-done.3
  17.0 0.5 collective-permute-done.3.other_sums
  17.5 1.9 %shard_map.213 = (bf16[16,256]{1,0:T(8,128)(2,1)S(1)}, bf16[16,32]{1,0:T(8,128)(2,1)S(1)}, f32[3,256,128]{2,1,0:T(8,128)S(1)}, f32[16,640]{1,0:T(8,128)S(1)}, f32[16,640]{1,0:T(8,128)S(1)}) custom-call(f32[8,896]{1,0:T(8,128)S(1)} %add.35.own_sums, f32[8,896]{1,0:T(8,128)S(1)} %collective-permute-done.3.other_sums, ...), custom_call_target="tpu_custom_call" | custom-call | tf_op jit(solution)/shard_map/pallas_call | solution.py:62
  19.4 0.2 collective-permute-start.4
  19.6 1.1 %collective-permute-done.4.refs_1_ = f32[16,640]{1,0:T(8,128)S(1)} collective-permute-done((f32[16,640]{1,0:T(8,128)S(1)}, f32[16,640]{1,0:T(8,128)S(1)}, u32[]{:S(2)}, u32[]{:S(2)}) %collective-permute-start.4) | collective-permute-done | bytes 40992 | tf_op jit(solution)/shard_map/ppermute | solution.py:26
  20.8 1.4 %collective-permute-start.5 = (f32[16,640]{1,0:T(8,128)S(1)}, f32[16,640]{1,0:T(8,128)S(1)}, u32[]{:S(2)}, u32[]{:S(2)}) collective-permute-start(f32[16,640]{1,0:T(8,128)S(1)} %shard_map.214.refs_0_), channel_id=1, source_target_pairs={{0,12},{1,13},{2,14},{3,15},{4,8},{5,9},{6,10},{7,11},{8,4},{9,5},... | collective-permute-start | bytes 122888 | tf_op jit(solution)/shard_map/ppermute | solution.py:26
  22.2 0.3 collective-permute-start.6
  22.5 1.9 %collective-permute-done.5.refs_1_ = f32[16,640]{1,0:T(8,128)S(1)} collective-permute-done((f32[16,640]{1,0:T(8,128)S(1)}, f32[16,640]{1,0:T(8,128)S(1)}, u32[]{:S(2)}, u32[]{:S(2)}) %collective-permute-start.5) | collective-permute-done | bytes 40992 | tf_op jit(solution)/shard_map/ppermute | solution.py:26
  24.4 1.3 %collective-permute-start.7 = (f32[16,640]{1,0:T(8,128)S(1)}, f32[16,640]{1,0:T(8,128)S(1)}, u32[]{:S(2)}, u32[]{:S(2)}) collective-permute-start(f32[16,640]{1,0:T(8,128)S(1)} %shard_map.214.refs_0_), channel_id=1, source_target_pairs={{0,24},{1,25},{2,26},{3,27},{4,28},{5,29},{6,30},{7,31},{8,16},{9,... | collective-permute-start | bytes 122888 | tf_op jit(solution)/shard_map/ppermute | solution.py:26
  25.7 1.9 %collective-permute-done.6.refs_2_ = f32[16,640]{1,0:T(8,128)S(1)} collective-permute-done((f32[16,640]{1,0:T(8,128)S(1)}, f32[16,640]{1,0:T(8,128)S(1)}, u32[]{:S(2)}, u32[]{:S(2)}) %collective-permute-start.6) | collective-permute-done | bytes 40992 | tf_op jit(solution)/shard_map/ppermute | solution.py:26
  27.6 2.6 %collective-permute-done.7.refs_3_ = f32[16,640]{1,0:T(8,128)S(1)} collective-permute-done((f32[16,640]{1,0:T(8,128)S(1)}, f32[16,640]{1,0:T(8,128)S(1)}, u32[]{:S(2)}, u32[]{:S(2)}) %collective-permute-start.7) | collective-permute-done | bytes 40992 | tf_op jit(solution)/shard_map/ppermute | solution.py:26
  30.2 0.2 shard_map.215.refs_0_
  30.4 2.5 %collective-permute-start.10 = (f32[16,640]{1,0:T(8,128)S(1)}, f32[16,640]{1,0:T(8,128)S(1)}, u32[]{:S(2)}, u32[]{:S(2)}) collective-permute-start(f32[16,640]{1,0:T(8,128)S(1)} %shard_map.215.refs_0_), channel_id=1, source_target_pairs={{0,3},{1,2},{2,1},{3,0},{4,7},{5,6},{6,5},{7,4},{8,11},{9,10},{10,... | collective-permute-start | bytes 122888 | tf_op jit(solution)/shard_map/ppermute | solution.py:26
  32.9 2.4 %collective-permute-done.10.refs_3_ = f32[16,640]{1,0:T(8,128)S(1)} collective-permute-done((f32[16,640]{1,0:T(8,128)S(1)}, f32[16,640]{1,0:T(8,128)S(1)}, u32[]{:S(2)}, u32[]{:S(2)}) %collective-permute-start.10) | collective-permute-done | bytes 40992 | tf_op jit(solution)/shard_map/ppermute | solution.py:26
  35.4 1.0 %collective-permute-done.8.refs_1_ = f32[16,640]{1,0:T(8,128)S(1)} collective-permute-done((f32[16,640]{1,0:T(8,128)S(1)}, f32[16,640]{1,0:T(8,128)S(1)}, u32[]{:S(2)}, u32[]{:S(2)}) %collective-permute-start.8) | collective-permute-done | bytes 40992 | tf_op jit(solution)/shard_map/ppermute | solution.py:26
  36.3 2.8 %collective-permute-done.9.refs_2_ = f32[16,640]{1,0:T(8,128)S(1)} collective-permute-done((f32[16,640]{1,0:T(8,128)S(1)}, f32[16,640]{1,0:T(8,128)S(1)}, u32[]{:S(2)}, u32[]{:S(2)}) %collective-permute-start.9) | collective-permute-done | bytes 40992 | tf_op jit(solution)/shard_map/ppermute | solution.py:26
  39.2 0.2 shard_map.216.refs_0_
  39.4 0.2 collective-permute-start.11
  39.5 0.3 shard_map.217
  39.8 0.8 %collective-permute-done.11.refs_1_ = f32[16,640]{1,0:T(8,128)S(1)} collective-permute-done((f32[16,640]{1,0:T(8,128)S(1)}, f32[16,640]{1,0:T(8,128)S(1)}, u32[]{:S(2)}, u32[]{:S(2)}) %collective-permute-start.11) | collective-permute-done | bytes 40992 | tf_op jit(solution)/shard_map/ppermute | solution.py:26
  40.6 0.7 %shard_map.218 = (f32[16,256]{1,0:T(8,128)S(1)}, f32[136,128]{1,0:T(8,128)S(1)}, f32[136,128]{1,0:T(8,128)S(1)}) custom-call(f32[16,640]{1,0:T(8,128)S(1)} %shard_map.216.refs_0_, f32[16,640]{1,0:T(8,128)S(1)} %collective-permute-done.11.refs_1_, f32[2,16,128]{2,1,0:T(8,128)S(1)} %get-tuple-element.45.refs_2_, f32[16,1024]{1,0:T(8,128)S(1)} %get-tuple-element.46.refs_3_, ...), custom_call_target="tpu_custom_call" | custom-call | tf_op jit(solution)/shard_map/pallas_call | solution.py:62
  41.4 0.2 collective-permute-start.15
  41.6 1.1 %collective-permute-done.15 = f32[136,128]{1,0:T(8,128)S(1)} collective-permute-done((f32[136,128]{1,0:T(8,128)S(1)}, f32[136,128]{1,0:T(8,128)S(1)}, u32[]{:S(2)}, u32[]{:S(2)}) %collective-permute-start.15) | collective-permute-done | bytes 69664 | tf_op jit(solution)/shard_map/ppermute | solution.py:26
  42.7 0.7 %collective-permute-start.16 = (f32[136,128]{1,0:T(8,128)S(1)}, f32[136,128]{1,0:T(8,128)S(1)}, u32[]{:S(2)}, u32[]{:S(2)}) collective-permute-start(f32[136,128]{1,0:T(8,128)S(1)} %add.36), channel_id=1, source_target_pairs={{0,12},{1,13},{2,14},{3,15},{4,8},{5,9},{6,10},{7,11},{8,4},{9,5},... | collective-permute-start | bytes 208904 | tf_op jit(solution)/shard_map/ppermute | solution.py:26
  43.4 1.0 %collective-permute-start.17 = (f32[136,128]{1,0:T(8,128)S(1)}, f32[136,128]{1,0:T(8,128)S(1)}, u32[]{:S(2)}, u32[]{:S(2)}) collective-permute-start(f32[136,128]{1,0:T(8,128)S(1)} %add.36), channel_id=1, source_target_pairs={{0,20},{1,21},{2,22},{3,23},{4,16},{5,17},{6,18},{7,19},{8,28},{9,... | collective-permute-start | bytes 208904 | tf_op jit(solution)/shard_map/ppermute | solution.py:26
  44.4 2.5 %collective-permute-start.18 = (f32[136,128]{1,0:T(8,128)S(1)}, f32[136,128]{1,0:T(8,128)S(1)}, u32[]{:S(2)}, u32[]{:S(2)}) collective-permute-start(f32[136,128]{1,0:T(8,128)S(1)} %add.36), channel_id=1, source_target_pairs={{0,24},{1,25},{2,26},{3,27},{4,28},{5,29},{6,30},{7,31},{8,16},{9,... | collective-permute-start | bytes 208904 | tf_op jit(solution)/shard_map/ppermute | solution.py:26
  46.9 4.4 %collective-permute-done.17 = f32[136,128]{1,0:T(8,128)S(1)} collective-permute-done((f32[136,128]{1,0:T(8,128)S(1)}, f32[136,128]{1,0:T(8,128)S(1)}, u32[]{:S(2)}, u32[]{:S(2)}) %collective-permute-start.17) | collective-permute-done | bytes 69664 | tf_op jit(solution)/shard_map/ppermute | solution.py:26
  51.3 0.9 %collective-permute-start.19 = (f32[136,128]{1,0:T(8,128)S(1)}, f32[136,128]{1,0:T(8,128)S(1)}, u32[]{:S(2)}, u32[]{:S(2)}) collective-permute-start(f32[136,128]{1,0:T(8,128)S(1)} %add_add_fusion.own), channel_id=1, source_target_pairs={{0,4},{1,5},{2,6},{3,7},{4,0},{5,1},{6,2},{7,3},{8,12},{9,13},{10,... | collective-permute-start | bytes 208904 | tf_op jit(solution)/shard_map/ppermute | solution.py:26
  52.2 0.9 %collective-permute-done.19.other = f32[136,128]{1,0:T(8,128)S(1)} collective-permute-done((f32[136,128]{1,0:T(8,128)S(1)}, f32[136,128]{1,0:T(8,128)S(1)}, u32[]{:S(2)}, u32[]{:S(2)}) %collective-permute-start.19) | collective-permute-done | bytes 69664 | tf_op jit(solution)/shard_map/ppermute | solution.py:26
  53.1 0.4 shard_map.219
  53.5 1.9 %collective-permute-start.20 = (f32[16,256]{1,0:T(8,128)S(1)}, f32[16,256]{1,0:T(8,128)S(1)}, u32[]{:S(2)}, u32[]{:S(2)}) collective-permute-start(f32[16,256]{1,0:T(8,128)S(1)} %shard_map.219), channel_id=1, source_target_pairs={{0,1},{1,0},{2,3},{3,2},{4,5},{5,4},{6,7},{7,6},{8,9},{9,8},{10,11... | collective-permute-start | bytes 49160 | tf_op jit(solution)/shard_map/ppermute | solution.py:26
  55.4 1.2 %collective-permute-start.21 = (f32[16,256]{1,0:T(8,128)S(1)}, f32[16,256]{1,0:T(8,128)S(1)}, u32[]{:S(2)}, u32[]{:S(2)}) collective-permute-start(f32[16,256]{1,0:T(8,128)S(1)} %shard_map.219), channel_id=1, source_target_pairs={{0,2},{1,3},{2,0},{3,1},{4,6},{5,7},{6,4},{7,5},{8,10},{9,11},{10,... | collective-permute-start | bytes 49160 | tf_op jit(solution)/shard_map/ppermute | solution.py:26
  56.6 0.4 collective-permute-start.22
  57.0 0.6 copy.23
  57.6 0.6 copy.24
  58.2 0.9 %collective-permute-done.21 = f32[16,256]{1,0:T(8,128)S(1)} collective-permute-done((f32[16,256]{1,0:T(8,128)S(1)}, f32[16,256]{1,0:T(8,128)S(1)}, u32[]{:S(2)}, u32[]{:S(2)}) %collective-permute-start.21) | collective-permute-done | bytes 16416 | tf_op jit(solution)/shard_map/ppermute | solution.py:26
  59.1 2.1 %collective-permute-done.22 = f32[16,256]{1,0:T(8,128)S(1)} collective-permute-done((f32[16,256]{1,0:T(8,128)S(1)}, f32[16,256]{1,0:T(8,128)S(1)}, u32[]{:S(2)}, u32[]{:S(2)}) %collective-permute-start.22) | collective-permute-done | bytes 16416 | tf_op jit(solution)/shard_map/ppermute | solution.py:26
  61.2 0.6 add_convert_fusion
  (29 shorter events, 0.4 us)
Async XLA Ops:
  2.1 1.4 %collective-permute-start = (f32[8,896]{1,0:T(8,128)S(1)}, f32[8,896]{1,0:T(8,128)S(1)}, u32[]{:S(2)}, u32[]{:S(2)}) collective-permute-start(f32[8,896]{1,0:T(8,128)S(1)} %get-tuple-element.29), channel_id=1, source_target_pairs={{0,4},{1,5},{2,6},{3,7},{4,0},{5,1},{6,2},{7,3},{8,12},{9,13},{10,... | collective-permute-start | bytes 86024 | tf_op jit(solution)/shard_map/ppermute | solution.py:26
  3.5 4.2 %collective-permute-start.1 = (f32[8,896]{1,0:T(8,128)S(1)}, f32[8,896]{1,0:T(8,128)S(1)}, u32[]{:S(2)}, u32[]{:S(2)}) collective-permute-start(f32[8,896]{1,0:T(8,128)S(1)} %add.33), channel_id=1, source_target_pairs={{0,12},{1,13},{2,14},{3,15},{4,8},{5,9},{6,10},{7,11},{8,4},{9,5},... | collective-permute-start | bytes 86024 | tf_op jit(solution)/shard_map/ppermute | solution.py:26
  7.8 6.3 %copy-start.5 = (s32[16]{0:T(128)S(1)}, s32[16]{0:T(128)}, u32[]{:S(2)}) copy-start(s32[16]{0:T(128)} %param.21) | copy-start | bytes 196
  7.8 8.4 %collective-permute-start.2 = (f32[8,896]{1,0:T(8,128)S(1)}, f32[8,896]{1,0:T(8,128)S(1)}, u32[]{:S(2)}, u32[]{:S(2)}) collective-permute-start(f32[8,896]{1,0:T(8,128)S(1)} %add.34.refs_0_), channel_id=1, source_target_pairs={{0,20},{1,21},{2,22},{3,23},{4,16},{5,17},{6,18},{7,19},{8,28},{9,... | collective-permute-start | bytes 86024 | tf_op jit(solution)/shard_map/ppermute | solution.py:26
  10.6 29.2 %collective-permute-start.12 = (f32[256,256]{1,0:T(8,128)S(1)}, f32[256,256]{1,0:T(8,128)S(1)}, u32[]{:S(2)}, u32[]{:S(2)}) collective-permute-start(f32[256,256]{1,0:T(8,128)S(1)} %get-tuple-element.49), channel_id=1, source_target_pairs={{0,1},{1,0},{2,3},{3,2},{4,5},{5,4},{6,7},{7,6},{8,9},{9,8},{10,11... | collective-permute-start | bytes 786440 | tf_op jit(solution)/shard_map/ppermute | solution.py:26
  12.1 27.7 %collective-permute-start.13 = (f32[256,256]{1,0:T(8,128)S(1)}, f32[256,256]{1,0:T(8,128)S(1)}, u32[]{:S(2)}, u32[]{:S(2)}) collective-permute-start(f32[256,256]{1,0:T(8,128)S(1)} %get-tuple-element.49), channel_id=1, source_target_pairs={{0,2},{1,3},{2,0},{3,1},{4,6},{5,7},{6,4},{7,5},{8,10},{9,11},{10,... | collective-permute-start | bytes 786440 | tf_op jit(solution)/shard_map/ppermute | solution.py:26
  13.6 26.2 %collective-permute-start.14 = (f32[256,256]{1,0:T(8,128)S(1)}, f32[256,256]{1,0:T(8,128)S(1)}, u32[]{:S(2)}, u32[]{:S(2)}) collective-permute-start(f32[256,256]{1,0:T(8,128)S(1)} %get-tuple-element.49), channel_id=1, source_target_pairs={{0,3},{1,2},{2,1},{3,0},{4,7},{5,6},{6,5},{7,4},{8,11},{9,10},{10,... | collective-permute-start | bytes 786440 | tf_op jit(solution)/shard_map/ppermute | solution.py:26
  16.2 0.7 %copy-start.3 = (f32[128]{0:T(128)S(1)}, f32[128]{0:T(128)}, u32[]{:S(2)}) copy-start(f32[128]{0:T(128)} %constant.5.clone) | copy-start | bytes 1540
  16.2 0.7 %copy-start.4 = (f32[128]{0:T(128)S(1)}, f32[128]{0:T(128)}, u32[]{:S(2)}) copy-start(f32[128]{0:T(128)} %constant.6) | copy-start | bytes 1540
  16.2 1.3 %collective-permute-start.3 = (f32[8,896]{1,0:T(8,128)S(1)}, f32[8,896]{1,0:T(8,128)S(1)}, u32[]{:S(2)}, u32[]{:S(2)}) collective-permute-start(f32[8,896]{1,0:T(8,128)S(1)} %add.35.own_sums), channel_id=1, source_target_pairs={{0,4},{1,5},{2,6},{3,7},{4,0},{5,1},{6,2},{7,3},{8,12},{9,13},{10,... | collective-permute-start | bytes 86024 | tf_op jit(solution)/shard_map/ppermute | solution.py:26
  19.3 21.3 %copy-start = (bf16[256,2048]{1,0:T(8,128)(2,1)S(1)}, bf16[256,2048]{1,0:T(8,128)(2,1)}, u32[]{:S(2)}) copy-start(bf16[256,2048]{1,0:T(8,128)(2,1)} %refs_6_.1) | copy-start | bytes 3145732
  19.4 1.3 %collective-permute-start.4 = (f32[16,640]{1,0:T(8,128)S(1)}, f32[16,640]{1,0:T(8,128)S(1)}, u32[]{:S(2)}, u32[]{:S(2)}) collective-permute-start(f32[16,640]{1,0:T(8,128)S(1)} %get-tuple-element.41), channel_id=1, source_target_pairs={{0,4},{1,5},{2,6},{3,7},{4,0},{5,1},{6,2},{7,3},{8,12},{9,13},{10,... | collective-permute-start | bytes 122888 | tf_op jit(solution)/shard_map/ppermute | solution.py:26
  20.8 3.6 %collective-permute-start.5 = (f32[16,640]{1,0:T(8,128)S(1)}, f32[16,640]{1,0:T(8,128)S(1)}, u32[]{:S(2)}, u32[]{:S(2)}) collective-permute-start(f32[16,640]{1,0:T(8,128)S(1)} %shard_map.214.refs_0_), channel_id=1, source_target_pairs={{0,12},{1,13},{2,14},{3,15},{4,8},{5,9},{6,10},{7,11},{8,4},{9,5},... | collective-permute-start | bytes 122888 | tf_op jit(solution)/shard_map/ppermute | solution.py:26
  22.2 5.4 %collective-permute-start.6 = (f32[16,640]{1,0:T(8,128)S(1)}, f32[16,640]{1,0:T(8,128)S(1)}, u32[]{:S(2)}, u32[]{:S(2)}) collective-permute-start(f32[16,640]{1,0:T(8,128)S(1)} %shard_map.214.refs_0_), channel_id=1, source_target_pairs={{0,20},{1,21},{2,22},{3,23},{4,16},{5,17},{6,18},{7,19},{8,28},{9,... | collective-permute-start | bytes 122888 | tf_op jit(solution)/shard_map/ppermute | solution.py:26
  24.4 5.8 %collective-permute-start.7 = (f32[16,640]{1,0:T(8,128)S(1)}, f32[16,640]{1,0:T(8,128)S(1)}, u32[]{:S(2)}, u32[]{:S(2)}) collective-permute-start(f32[16,640]{1,0:T(8,128)S(1)} %shard_map.214.refs_0_), channel_id=1, source_target_pairs={{0,24},{1,25},{2,26},{3,27},{4,28},{5,29},{6,30},{7,31},{8,16},{9,... | collective-permute-start | bytes 122888 | tf_op jit(solution)/shard_map/ppermute | solution.py:26
  30.4 5.0 %collective-permute-start.10 = (f32[16,640]{1,0:T(8,128)S(1)}, f32[16,640]{1,0:T(8,128)S(1)}, u32[]{:S(2)}, u32[]{:S(2)}) collective-permute-start(f32[16,640]{1,0:T(8,128)S(1)} %shard_map.215.refs_0_), channel_id=1, source_target_pairs={{0,3},{1,2},{2,1},{3,0},{4,7},{5,6},{6,5},{7,4},{8,11},{9,10},{10,... | collective-permute-start | bytes 122888 | tf_op jit(solution)/shard_map/ppermute | solution.py:26
  32.9 3.4 %collective-permute-start.8 = (f32[16,640]{1,0:T(8,128)S(1)}, f32[16,640]{1,0:T(8,128)S(1)}, u32[]{:S(2)}, u32[]{:S(2)}) collective-permute-start(f32[16,640]{1,0:T(8,128)S(1)} %shard_map.215.refs_0_), channel_id=1, source_target_pairs={{0,5},{1,4},{2,7},{3,6},{4,1},{5,0},{6,3},{7,2},{8,13},{9,12},{10,... | collective-permute-start | bytes 122888 | tf_op jit(solution)/shard_map/ppermute | solution.py:26
  35.4 3.8 %collective-permute-start.9 = (f32[16,640]{1,0:T(8,128)S(1)}, f32[16,640]{1,0:T(8,128)S(1)}, u32[]{:S(2)}, u32[]{:S(2)}) collective-permute-start(f32[16,640]{1,0:T(8,128)S(1)} %shard_map.215.refs_0_), channel_id=1, source_target_pairs={{0,6},{1,7},{2,4},{3,5},{4,2},{5,3},{6,0},{7,1},{8,14},{9,15},{10,... | collective-permute-start | bytes 122888 | tf_op jit(solution)/shard_map/ppermute | solution.py:26
  39.4 1.3 %collective-permute-start.11 = (f32[16,640]{1,0:T(8,128)S(1)}, f32[16,640]{1,0:T(8,128)S(1)}, u32[]{:S(2)}, u32[]{:S(2)}) collective-permute-start(f32[16,640]{1,0:T(8,128)S(1)} %shard_map.216.refs_0_), channel_id=1, source_target_pairs={{0,4},{1,5},{2,6},{3,7},{4,0},{5,1},{6,2},{7,3},{8,12},{9,13},{10,... | collective-permute-start | bytes 122888 | tf_op jit(solution)/shard_map/ppermute | solution.py:26
  39.5 1.1 %copy-start.2 = (bf16[4,64,256]{2,1,0:T(8,128)(2,1)S(1)}, bf16[4,64,256]{2,1,0:T(8,128)(2,1)}, u32[]{:S(2)}) copy-start(bf16[4,64,256]{2,1,0:T(8,128)(2,1)} %param.34) | copy-start | bytes 393220
  40.6 12.5 %copy-start.1 = (bf16[2048,256]{1,0:T(8,128)(2,1)S(1)}, bf16[2048,256]{1,0:T(8,128)(2,1)}, u32[]{:S(2)}) copy-start(bf16[2048,256]{1,0:T(8,128)(2,1)} %w_out.1) | copy-start | bytes 3145732
  41.4 1.3 %collective-permute-start.15 = (f32[136,128]{1,0:T(8,128)S(1)}, f32[136,128]{1,0:T(8,128)S(1)}, u32[]{:S(2)}, u32[]{:S(2)}) collective-permute-start(f32[136,128]{1,0:T(8,128)S(1)} %get-tuple-element.52), channel_id=1, source_target_pairs={{0,4},{1,5},{2,6},{3,7},{4,0},{5,1},{6,2},{7,3},{8,12},{9,13},{10,... | collective-permute-start | bytes 208904 | tf_op jit(solution)/shard_map/ppermute | solution.py:26
  42.7 4.2 %collective-permute-start.16 = (f32[136,128]{1,0:T(8,128)S(1)}, f32[136,128]{1,0:T(8,128)S(1)}, u32[]{:S(2)}, u32[]{:S(2)}) collective-permute-start(f32[136,128]{1,0:T(8,128)S(1)} %add.36), channel_id=1, source_target_pairs={{0,12},{1,13},{2,14},{3,15},{4,8},{5,9},{6,10},{7,11},{8,4},{9,5},... | collective-permute-start | bytes 208904 | tf_op jit(solution)/shard_map/ppermute | solution.py:26
  43.4 7.8 %collective-permute-start.17 = (f32[136,128]{1,0:T(8,128)S(1)}, f32[136,128]{1,0:T(8,128)S(1)}, u32[]{:S(2)}, u32[]{:S(2)}) collective-permute-start(f32[136,128]{1,0:T(8,128)S(1)} %add.36), channel_id=1, source_target_pairs={{0,20},{1,21},{2,22},{3,23},{4,16},{5,17},{6,18},{7,19},{8,28},{9,... | collective-permute-start | bytes 208904 | tf_op jit(solution)/shard_map/ppermute | solution.py:26
  44.4 6.9 %collective-permute-start.18 = (f32[136,128]{1,0:T(8,128)S(1)}, f32[136,128]{1,0:T(8,128)S(1)}, u32[]{:S(2)}, u32[]{:S(2)}) collective-permute-start(f32[136,128]{1,0:T(8,128)S(1)} %add.36), channel_id=1, source_target_pairs={{0,24},{1,25},{2,26},{3,27},{4,28},{5,29},{6,30},{7,31},{8,16},{9,... | collective-permute-start | bytes 208904 | tf_op jit(solution)/shard_map/ppermute | solution.py:26
  51.3 1.8 %collective-permute-start.19 = (f32[136,128]{1,0:T(8,128)S(1)}, f32[136,128]{1,0:T(8,128)S(1)}, u32[]{:S(2)}, u32[]{:S(2)}) collective-permute-start(f32[136,128]{1,0:T(8,128)S(1)} %add_add_fusion.own), channel_id=1, source_target_pairs={{0,4},{1,5},{2,6},{3,7},{4,0},{5,1},{6,2},{7,3},{8,12},{9,13},{10,... | collective-permute-start | bytes 208904 | tf_op jit(solution)/shard_map/ppermute | solution.py:26
  53.5 4.7 %collective-permute-start.20 = (f32[16,256]{1,0:T(8,128)S(1)}, f32[16,256]{1,0:T(8,128)S(1)}, u32[]{:S(2)}, u32[]{:S(2)}) collective-permute-start(f32[16,256]{1,0:T(8,128)S(1)} %shard_map.219), channel_id=1, source_target_pairs={{0,1},{1,0},{2,3},{3,2},{4,5},{5,4},{6,7},{7,6},{8,9},{9,8},{10,11... | collective-permute-start | bytes 49160 | tf_op jit(solution)/shard_map/ppermute | solution.py:26
  55.4 3.7 %collective-permute-start.21 = (f32[16,256]{1,0:T(8,128)S(1)}, f32[16,256]{1,0:T(8,128)S(1)}, u32[]{:S(2)}, u32[]{:S(2)}) collective-permute-start(f32[16,256]{1,0:T(8,128)S(1)} %shard_map.219), channel_id=1, source_target_pairs={{0,2},{1,3},{2,0},{3,1},{4,6},{5,7},{6,4},{7,5},{8,10},{9,11},{10,... | collective-permute-start | bytes 49160 | tf_op jit(solution)/shard_map/ppermute | solution.py:26
  56.6 4.6 %collective-permute-start.22 = (f32[16,256]{1,0:T(8,128)S(1)}, f32[16,256]{1,0:T(8,128)S(1)}, u32[]{:S(2)}, u32[]{:S(2)}) collective-permute-start(f32[16,256]{1,0:T(8,128)S(1)} %shard_map.219), channel_id=1, source_target_pairs={{0,3},{1,2},{2,1},{3,0},{4,7},{5,6},{6,5},{7,4},{8,11},{9,10},{10,... | collective-permute-start | bytes 49160 | tf_op jit(solution)/shard_map/ppermute | solution.py:26
